TPU v7x, 256 devices: a 4x2x16 block of a 4x16x16 slice. The times are simulated.
256 devices in a mesh: grp: 2 (over y), tp: 16 (over z), dp: 8 (over x, core).
Axes of the slice: x: 4, y: 2, z: 16, core: 2. Of those that a mesh axis runs over, the one named last changes fastest.
The devices are a block of a 4x16x16 slice.
Arguments:
- skip_path_activations: bfloat16 [256, 8, 4096], P('grp', None, 'dp'), parts along dimension 0
- novel_lengths_per_sequence: int32 [256], P(('grp', 'dp')), parts along dimension 0, may hold values from 1 to 8, 512 in all
- input_normalizer_scales: bfloat16 [2, 4096], P(None, 'dp'), may hold values from 0.099609375 to 1.8984375
- question_projector: bfloat16 [2, 4096, 2048], P(None, 'dp', 'tp'), may hold values from -0.09375 to 0.09375
- lookup_projector: bfloat16 [2, 4096, 2048], P(None, 'dp', 'tp'), may hold values from -0.09375 to 0.09375
- payload_projector: bfloat16 [2, 4096, 4096], P(None, 'dp', 'tp'), may hold values from -0.09375 to 0.09375
- emitted_valve_projector: bfloat16 [2, 4096, 4096], P(None, 'dp', 'tp'), may hold values from -0.09375 to 0.09375
- keeping_valve_projector: bfloat16 [2, 4096, 2048], P(None, 'dp', 'tp'), may hold values from -0.09375 to 0.09375
- keeping_valve_shift: float32 [2, 2048], P(None, 'tp'), may hold values from -3 to 6
- additional_dwindle_exponent: float32 [256, 8, 16], P(('grp', 'dp'), None, 'tp'), parts along dimension 0, may hold values from -0.7 to 0
- headwise_normalizer_scales: bfloat16 [2, 256], replicated, may hold values from 0.099609375 to 1.8984375
- closing_projector: bfloat16 [2, 4096, 4096], P(None, 'tp', 'dp'), may hold values from -0.1875 to 0.1875
- earlier_recurrence_grid: float32 [2, 256, 16, 128, 256], P(None, ('grp', 'dp'), 'tp'), parts along dimension 1, may hold values from -6 to 6
Outputs:
- stream_out: bfloat16 [256, 8, 4096], P('grp', None, 'dp'), parts along dimension 0
- state_out: float32 [2, 256, 16, 128, 256], P(None, ('grp', 'dp'), 'tp'), parts along dimension 1
There are 2 independent parts, one for each index of `grp`. A program takes and returns all parts, laid end to end along the dimension named above; an argument that names none is the same for every part. Nothing has to cross between parts.
Inputs may be any that keep to these rules, and one draw needn't show every extreme that they name: `novel_lengths_per_sequence`: each sequence has 1 to 8 live token slots, the first ones; some sequence has 8. In each group the live slots of its 128 sequences add up to half of 128 times 8.
All inputs are finite; a program needn't handle non-finite values.
Results may differ from a plain program's by a relative error of at most 0.024.
Values may be sent and summed in bfloat16 or wider, within the bound.
No kernel may reach another device: no remote copies, remote signals or barrier semaphores. Data moves between devices by JAX's collectives and lax.ppermute only.
A program may use at most 64 MiB of HBM per device.

v0:
```python
import jax
import jax.numpy as jnp
from jax import lax
from jax.sharding import PartitionSpec as P

LAYERS = 2


EPS = 1e-06
TAU = 16.0


def copy_for_each(x, axis):
    count = lax.axis_size(axis)
    return lax.all_to_all(jnp.broadcast_to(x[None], (count, *x.shape)), axis, 0, 0, tiled=True)


def of_everyone(x, axis):
    everything = copy_for_each(x, axis)
    return jnp.sum(everything, axis=0)


def cut_along(x, dim, count):
    before, after = (x.shape[:dim], x.shape[dim + 1 :])
    return jnp.moveaxis(x.reshape(*before, count, -1, *after), dim, 0)


def summed_on_arrival(x, axis, dim):
    tiles = cut_along(x, dim, lax.axis_size(axis))
    arrived = lax.all_to_all(tiles, axis, split_axis=0, concat_axis=0, tiled=True)
    return arrived.astype(jnp.float32).sum(axis=0)


def laid_out(tiles, dim):
    dims = list(tiles.shape[1:])
    dims[dim] *= tiles.shape[0]
    return jnp.moveaxis(tiles, 0, dim).reshape(dims)


def collect(x, axis, dim):
    return laid_out(copy_for_each(x, axis), dim)


def scaled_rms(values_f, gain):
    return (
        values_f
        * lax.rsqrt(jnp.mean(values_f * values_f, axis=-1, keepdims=True) + EPS)
        * gain.astype(jnp.float32)
    )


def round_trip(values_f):
    return lax.optimization_barrier(values_f.astype(jnp.bfloat16)).astype(jnp.float32)


def advance(query_rows, key_rows, value_rows, fade_log_amount, carried):
    steps_n = query_rows.shape[1]
    cumulative = jnp.cumsum(fade_log_amount, axis=1)
    spread = cumulative[:, :, None] - cumulative[:, None, :]
    causal = jnp.tril(jnp.ones((steps_n, steps_n), dtype=bool))
    decay_mat = jnp.exp(jnp.where(causal[None, :, :, None, None], spread, -jnp.inf))
    scores = jnp.einsum("sihd,sjhd,sijhd->shij", query_rows, key_rows, decay_mat)
    within = jnp.einsum("shij,sjhv->sihv", scores, value_rows)
    carried_part = jnp.einsum("sihd,shdv->sihv", query_rows * jnp.exp(cumulative), carried)
    final_log = cumulative[:, -1]
    weighted = key_rows * jnp.exp(final_log[:, None] - cumulative)
    updated = jnp.exp(final_log)[..., None] * carried + jnp.einsum(
        "sjhd,sjhv->shdv", weighted, value_rows
    )
    return (within + carried_part, updated)


def shards(
    skip_path_activations,
    novel_lengths_per_sequence,
    input_normalizer_scales,
    question_projector,
    lookup_projector,
    payload_projector,
    emitted_valve_projector,
    keeping_valve_projector,
    keeping_valve_shift,
    additional_dwindle_exponent,
    headwise_normalizer_scales,
    closing_projector,
    earlier_recurrence_grid,
):
    number_of_streams, number_of_iterations, shard_breadth = skip_path_activations.shape
    number_of_lines = number_of_streams * number_of_iterations
    local_seqs = novel_lengths_per_sequence.shape[0]
    local_rows = local_seqs * number_of_iterations
    existing_attender_list = additional_dwindle_exponent.shape[2]
    key_dim = earlier_recurrence_grid.shape[3]
    value_dim = earlier_recurrence_grid.shape[4]
    key_cols = existing_attender_list * key_dim
    value_cols = existing_attender_list * value_dim
    full_width = shard_breadth * lax.axis_size("dp")
    ongoing = skip_path_activations.reshape(number_of_lines, shard_breadth)
    live_entry_indicator = (
        lax.broadcasted_iota(jnp.int32, (local_seqs, number_of_iterations), 1)
        < novel_lengths_per_sequence[:, None]
    ).astype(jnp.float32)
    new_states = []
    for block_index in range(LAYERS):
        stream_f = ongoing.astype(jnp.float32)
        square_sum = of_everyone(jnp.sum(stream_f * stream_f, axis=1), "dp")
        normed = (
            stream_f
            * lax.rsqrt(square_sum / full_width + EPS)[:, None]
            * input_normalizer_scales[block_index].astype(jnp.float32)
        ).astype(jnp.bfloat16)
        matrices = (
            question_projector[block_index],
            lookup_projector[block_index],
            payload_projector[block_index],
            emitted_valve_projector[block_index],
            keeping_valve_projector[block_index],
        )
        summed = summed_on_arrival(
            jnp.concatenate(
                [
                    jnp.dot(normed, matrix, preferred_element_type=jnp.float32)
                    for matrix in matrices
                ],
                axis=1,
            ).astype(jnp.bfloat16),
            "dp",
            0,
        )
        query_rows = round_trip(summed[:, :key_cols]) * key_dim ** (-0.5)
        key_rows = round_trip(summed[:, key_cols : 2 * key_cols])
        value_rows = round_trip(summed[:, 2 * key_cols : 2 * key_cols + value_cols])
        gate_rows = round_trip(summed[:, 2 * key_cols + value_cols : 2 * key_cols + 2 * value_cols])
        logits = summed[:, 2 * key_cols + 2 * value_cols :]
        fade_log_amount = (
            jax.nn.log_sigmoid(logits + keeping_valve_shift[block_index]) / TAU
        ).reshape(local_seqs, number_of_iterations, existing_attender_list, key_dim)
        fade_log_amount = (
            fade_log_amount + additional_dwindle_exponent[..., None]
        ) * live_entry_indicator[:, :, None, None]
        key_rows = (
            key_rows.reshape(local_seqs, number_of_iterations, existing_attender_list, key_dim)
            * live_entry_indicator[:, :, None, None]
        )
        output, updated = advance(
            query_rows.reshape(local_seqs, number_of_iterations, existing_attender_list, key_dim),
            key_rows,
            value_rows.reshape(local_seqs, number_of_iterations, existing_attender_list, value_dim),
            fade_log_amount,
            earlier_recurrence_grid[block_index],
        )
        new_states.append(updated)
        normed_out = scaled_rms(output, headwise_normalizer_scales[block_index]).reshape(
            local_rows, value_cols
        )
        gated_rows = (
            normed_out * jax.nn.silu(gate_rows) * live_entry_indicator.reshape(local_rows, 1)
        ).astype(jnp.bfloat16)
        out_matrix = closing_projector[block_index]
        partial_value = jnp.dot(
            collect(gated_rows, "dp", 0), out_matrix, preferred_element_type=jnp.float32
        )
        share_part = summed_on_arrival(partial_value.astype(jnp.bfloat16), "tp", 1)
        span_cols = share_part.shape[1]
        own_columns = lax.dynamic_slice_in_dim(
            ongoing, lax.axis_index("tp") * span_cols, span_cols, 1
        )
        joined = (own_columns.astype(jnp.float32) + share_part).astype(jnp.bfloat16)
        ongoing = collect(joined, "tp", 1)
    return (
        ongoing.reshape(number_of_streams, number_of_iterations, shard_breadth),
        jnp.stack(new_states, axis=0),
    )


def solution(mesh):
    in_specs = (
        P("grp", None, "dp"),
        P(("grp", "dp")),
        P(None, "dp"),
        P(None, "dp", "tp"),
        P(None, "dp", "tp"),
        P(None, "dp", "tp"),
        P(None, "dp", "tp"),
        P(None, "dp", "tp"),
        P(None, "tp"),
        P(("grp", "dp"), None, "tp"),
        P(),
        P(None, "tp", "dp"),
        P(None, ("grp", "dp"), "tp", None, None),
    )
    out_specs = (P("grp", None, "dp"), P(None, ("grp", "dp"), "tp", None, None))
    return jax.shard_map(shards, mesh=mesh, in_specs=in_specs, out_specs=out_specs, check_vma=False)
```

profile of v0, /device:TPU:40, one launch (start us, length us, event | category | flops | bytes accessed | tf_op | source)
XLA Modules:
  0.0 386.3 jit_solution(1532063494647939995)
XLA Ops:
  0.7 1.6 fusion
  2.3 0.6 broadcast_in_dim.36
  3.0 4.6 %all-to-all-start = ((f32[8,1,1024]{2,1,0:T(1,128)}), f32[8,1,1024]{2,1,0:T(1,128)S(1)}, u32[]{:S(2)}, u32[]{:S(2)}) async-start(f32[8,1,1024]{2,1,0:T(1,128)} %broadcast_in_dim.36), calls=%async_computation | async-start | bytes 65536 | tf_op jit(solution)/shard_map/all_to_all | solution.py:15
  7.6 0.7 slice_convert_fusion
  8.3 4.8 %all-to-all-done = f32[8,1,1024]{2,1,0:T(1,128)S(1)} async-done(((f32[8,1,1024]{2,1,0:T(1,128)}), f32[8,1,1024]{2,1,0:T(1,128)S(1)}, u32[]{:S(2)}, u32[]{:S(2)}) %all-to-all-start) | async-done | bytes 32800 | tf_op jit(solution)/shard_map/all_to_all | solution.py:15
  13.2 0.3 fusion.2
  13.5 0.5 convolution_convert_fusion.10
  14.0 0.2 copy.148
  14.2 0.5 convolution_convert_fusion.11
  14.7 0.2 copy.147
  14.9 0.7 constant_dynamic-update-slice_fusion.1
  15.6 0.7 constant_dynamic-update-slice_fusion
  16.3 2.2 fusion.11
  18.5 1.2 fusion.10
  19.8 1.1 fusion.12
  20.9 3.9 %all-to-all-start.1 = ((bf16[8,128,896]{2,1,0:T(8,128)(2,1)}), bf16[8,128,896]{2,1,0:T(8,128)(2,1)S(1)}, u32[]{:S(2)}, u32[]{:S(2)}) async-start(bf16[8,128,896]{2,1,0:T(8,128)(2,1)} %fusion.12), calls=%async_computation.1 | async-start | bytes 3670016 | tf_op jit(solution)/shard_map/all_to_all | solution.py:30
  25.2 23.8 %all-to-all-done.1 = bf16[8,128,896]{2,1,0:T(8,128)(2,1)S(1)} async-done(((bf16[8,128,896]{2,1,0:T(8,128)(2,1)}), bf16[8,128,896]{2,1,0:T(8,128)(2,1)S(1)}, u32[]{:S(2)}, u32[]{:S(2)}) %all-to-all-start.1) | async-done | bytes 1835040 | tf_op jit(solution)/shard_map/all_to_all | solution.py:30
  49.0 0.3 convert_reduce_fusion.1
  49.6 1.8 fusion.15
  51.5 0.2 select_exponential_fusion.1
  51.6 0.2 fusion.19
  51.9 0.3 multiply_reduce_fusion.1
  52.4 12.8 %all_to_all.52 = bf16[8,128,256]{2,1,0:T(8,128)(2,1)S(1)} all-to-all(bf16[8,128,256]{2,1,0:T(8,128)(2,1)S(1)} %broadcast_in_dim.39), channel_id=1, replica_groups=mesh['grp'=2,'tp'=16,'dp'=8] {'dp'}, dimensions={0} | all-to-all | bytes 1048576 | tf_op jit(solution)/shard_map/all_to_all | solution.py:15
  65.2 1.5 convolution_convert_fusion.1
  66.7 24.0 %all-to-all-start.3 = ((bf16[16,1024,32]{1,2,0:T(8,128)(2,1)}), bf16[16,1024,32]{1,2,0:T(8,128)(2,1)S(1)}, u32[]{:S(2)}, u32[]{:S(2)}) async-start(bf16[16,1024,32]{1,2,0:T(8,128)(2,1)} %bitcast.40), calls=%async_computation.3 | async-start | bytes 2097152 | tf_op jit(solution)/shard_map/all_to_all | solution.py:30
  90.6 0.1 constant_dynamic-slice_fusion
  90.8 0.1 copy.184
  90.9 49.0 %all-to-all-done.3 = bf16[16,1024,32]{1,2,0:T(8,128)(2,1)S(1)} async-done(((bf16[16,1024,32]{1,2,0:T(8,128)(2,1)}), bf16[16,1024,32]{1,2,0:T(8,128)(2,1)S(1)}, u32[]{:S(2)}, u32[]{:S(2)}) %all-to-all-start.3) | async-done | bytes 1048608 | tf_op jit(solution)/shard_map/all_to_all | solution.py:30
  140.0 0.2 convert_reduce_fusion.3
  140.2 0.1 broadcast_in_dim.40
  140.3 59.5 %all_to_all.53 = bf16[16,1024,32]{1,2,0:T(8,128)(2,1)S(1)} all-to-all(bf16[16,1024,32]{1,2,0:T(8,128)(2,1)S(1)} %broadcast_in_dim.40), channel_id=1, replica_groups=mesh['grp'=2,'tp'=16,'dp'=8] {'tp'}, dimensions={0} | all-to-all | bytes 2097152 | tf_op jit(solution)/shard_map/all_to_all | solution.py:15
  199.9 0.2 fusion.3
  200.1 0.6 broadcast_in_dim.41
  200.7 3.5 all-to-all-start.5
  204.4 5.1 %all-to-all-done.5 = f32[8,1,1024]{2,1,0:T(1,128)S(1)} async-done(((f32[8,1,1024]{2,1,0:T(1,128)}), f32[8,1,1024]{2,1,0:T(1,128)S(1)}, u32[]{:S(2)}, u32[]{:S(2)}) %all-to-all-start.5) | async-done | bytes 32800 | tf_op jit(solution)/shard_map/all_to_all | solution.py:15
  209.6 0.3 fusion.5
  209.8 0.3 copy.191
  210.1 0.7 copy.153
  210.8 1.4 convolution_convert_fusion.7
  212.2 1.4 convolution_convert_fusion.8
  213.6 0.2 copy.162
  213.8 0.2 copy.161
  214.1 1.4 fusion.9
  215.6 0.4 fusion.8
  216.0 0.5 fusion.13
  216.6 26.9 %all_to_all.54 = bf16[8,128,896]{2,1,0:T(8,128)(2,1)S(1)} all-to-all(bf16[8,128,896]{2,1,0:T(8,128)(2,1)S(1)} %fusion.13), channel_id=1, replica_groups=mesh['grp'=2,'tp'=16,'dp'=8] {'dp'}, dimensions={0} | all-to-all | bytes 3670016 | tf_op jit(solution)/shard_map/all_to_all | solution.py:30
  243.5 0.3 convert_reduce_fusion
  244.1 1.8 fusion.14
  246.0 0.2 select_exponential_fusion
  246.1 0.2 fusion.18
  246.4 0.3 multiply_reduce_fusion
  246.8 13.0 %all_to_all.55 = bf16[8,128,256]{2,1,0:T(8,128)(2,1)S(1)} all-to-all(bf16[8,128,256]{2,1,0:T(8,128)(2,1)S(1)} %broadcast_in_dim.42), channel_id=1, replica_groups=mesh['grp'=2,'tp'=16,'dp'=8] {'dp'}, dimensions={0} | all-to-all | bytes 1048576 | tf_op jit(solution)/shard_map/all_to_all | solution.py:15
  259.9 0.5 convolution_convert_fusion
  260.4 57.2 %all_to_all.56 = bf16[16,1024,32]{1,2,0:T(8,128)(2,1)S(1)} all-to-all(bf16[16,1024,32]{1,2,0:T(8,128)(2,1)S(1)} %bitcast.245), channel_id=1, replica_groups=mesh['grp'=2,'tp'=16,'dp'=8] {'tp'}, dimensions={0} | all-to-all | bytes 2097152 | tf_op jit(solution)/shard_map/all_to_all | solution.py:30
  317.5 0.2 convert_reduce_fusion.2
  317.7 1.1 broadcast_in_dim.43
  318.8 6.6 %all-to-all-start.9 = ((bf16[16,1024,32]{1,2,0:T(8,128)(2,1)}), bf16[16,1024,32]{1,2,0:T(8,128)(2,1)S(1)}, u32[]{:S(2)}, u32[]{:S(2)}) async-start(bf16[16,1024,32]{1,2,0:T(8,128)(2,1)} %broadcast_in_dim.43), calls=%async_computation.9 | async-start | bytes 2097152 | tf_op jit(solution)/shard_map/all_to_all | solution.py:15
  325.5 2.6 add_bitcast_fusion.1
  328.1 0.2 copy-done
  328.3 1.1 add_bitcast_fusion
  329.4 2.4 maximum_bitcast_fusion
  331.8 42.9 %all-to-all-done.9 = bf16[16,1024,32]{1,2,0:T(8,128)(2,1)S(1)} async-done(((bf16[16,1024,32]{1,2,0:T(8,128)(2,1)}), bf16[16,1024,32]{1,2,0:T(8,128)(2,1)S(1)}, u32[]{:S(2)}, u32[]{:S(2)}) %all-to-all-start.9) | async-done | bytes 1048608 | tf_op jit(solution)/shard_map/all_to_all | solution.py:15
  374.7 4.8 %copy.164 = bf16[1024,16,32]{2,1,0:T(8,128)(2,1)} copy(bf16[1024,16,32]{0,2,1:T(8,128)(2,1)S(1)} %bitcast.244) | data formatting | bytes 2097152 | tf_op jit(solution)/shard_map/transpose | solution.py:37
  379.5 6.8 %reshape_reshape.3 = bf16[128,8,512]{2,1,0:T(8,128)(2,1)} reshape(bf16[1024,16,32]{2,1,0:T(8,128)(2,1)} %copy.164) | data formatting | bytes 2097152 | tf_op jit(solution)/shard_map/reshape;reshape | solution.py:171
  (71 shorter events, 1.8 us)
Async XLA Ops:
  0.6 12.5 %copy-start.1 = (bf16[128,8,512]{2,1,0:T(8,128)(2,1)S(1)}, bf16[128,8,512]{2,1,0:T(8,128)(2,1)}, u32[]{:S(2)}) copy-start(bf16[128,8,512]{2,1,0:T(8,128)(2,1)} %param.13) | copy-start | bytes 3145732
  0.6 12.9 %copy-start.4 = (bf16[2,512,128]{2,1,0:T(8,128)(2,1)S(1)}, bf16[2,512,128]{2,1,0:T(8,128)(2,1)}, u32[]{:S(2)}) copy-start(bf16[2,512,128]{2,1,0:T(8,128)(2,1)} %param.17) | copy-start | bytes 786436
  3.0 10.0 %all-to-all-start = ((f32[8,1,1024]{2,1,0:T(1,128)}), f32[8,1,1024]{2,1,0:T(1,128)S(1)}, u32[]{:S(2)}, u32[]{:S(2)}) async-start(f32[8,1,1024]{2,1,0:T(1,128)} %broadcast_in_dim.36), calls=%async_computation | async-start | bytes 65536 | tf_op jit(solution)/shard_map/all_to_all | solution.py:15
  13.1 1.1 copy-start.5
  14.9 3.7 copy-start.13
  16.3 3.5 copy-start.6
  20.9 4.0 %copy-start.12 = (s32[16]{0:T(128)S(1)}, s32[16]{0:T(128)}, u32[]{:S(2)}) copy-start(s32[16]{0:T(128)} %param.14) | copy-start | bytes 196
  20.9 4.1 %copy-start.9 = (f32[16,8,1]{0,2,1:T(1,128)S(1)}, f32[16,8,1]{0,2,1:T(1,128)}, u32[]{:S(2)}) copy-start(f32[16,8,1]{0,2,1:T(1,128)} %param.22) | copy-start | bytes 1540
  20.9 4.2 %copy-start.11 = (f32[2,128]{1,0:T(2,128)S(1)}, f32[2,128]{1,0:T(2,128)}, u32[]{:S(2)}) copy-start(f32[2,128]{1,0:T(2,128)} %param.21) | copy-start | bytes 3076
  20.9 4.2 %copy-start.10 = (bf16[2,256]{1,0:T(2,128)(2,1)S(1)}, bf16[2,256]{1,0:T(2,128)(2,1)}, u32[]{:S(2)}) copy-start(bf16[2,256]{1,0:T(2,128)(2,1)} %param.23) | copy-start | bytes 3076
  20.9 28.1 %all-to-all-start.1 = ((bf16[8,128,896]{2,1,0:T(8,128)(2,1)}), bf16[8,128,896]{2,1,0:T(8,128)(2,1)S(1)}, u32[]{:S(2)}, u32[]{:S(2)}) async-start(bf16[8,128,896]{2,1,0:T(8,128)(2,1)} %fusion.12), calls=%async_computation.1 | async-start | bytes 3670016 | tf_op jit(solution)/shard_map/all_to_all | solution.py:30
  51.5 13.7 %copy-start.2 = (bf16[2,256,512]{2,1,0:T(8,128)(2,1)S(1)}, bf16[2,256,512]{2,1,0:T(8,128)(2,1)}, u32[]{:S(2)}) copy-start(bf16[2,256,512]{2,1,0:T(8,128)(2,1)} %param.24) | copy-start | bytes 1572868
  66.7 73.3 %all-to-all-start.3 = ((bf16[16,1024,32]{1,2,0:T(8,128)(2,1)}), bf16[16,1024,32]{1,2,0:T(8,128)(2,1)S(1)}, u32[]{:S(2)}, u32[]{:S(2)}) async-start(bf16[16,1024,32]{1,2,0:T(8,128)(2,1)} %bitcast.40), calls=%async_computation.3 | async-start | bytes 2097152 | tf_op jit(solution)/shard_map/all_to_all | solution.py:30
  140.2 64.1 %copy-start.8 = (bf16[2,512]{1,0:T(2,128)(2,1)S(1)}, bf16[2,512]{1,0:T(2,128)(2,1)}, u32[]{:S(2)}) copy-start(bf16[2,512]{1,0:T(2,128)(2,1)} %param.15) | copy-start | bytes 6148
  200.7 8.8 %all-to-all-start.5 = ((f32[8,1,1024]{2,1,0:T(1,128)}), f32[8,1,1024]{2,1,0:T(1,128)S(1)}, u32[]{:S(2)}, u32[]{:S(2)}) async-start(f32[8,1,1024]{2,1,0:T(1,128)} %broadcast_in_dim.41), calls=%async_computation.5 | async-start | bytes 65536 | tf_op jit(solution)/shard_map/all_to_all | solution.py:15
  214.0 1.6 copy-start.14
  214.1 1.9 copy-start.7
  245.9 13.9 %copy-start.3 = (bf16[2,256,512]{2,1,0:T(8,128)(2,1)S(1)}, bf16[2,256,512]{2,1,0:T(8,128)(2,1)}, u32[]{:S(2)}) copy-start(bf16[2,256,512]{2,1,0:T(8,128)(2,1)} %param.24) | copy-start | bytes 1572868
  318.8 55.9 %all-to-all-start.9 = ((bf16[16,1024,32]{1,2,0:T(8,128)(2,1)}), bf16[16,1024,32]{1,2,0:T(8,128)(2,1)S(1)}, u32[]{:S(2)}, u32[]{:S(2)}) async-start(bf16[16,1024,32]{1,2,0:T(8,128)(2,1)} %broadcast_in_dim.43), calls=%async_computation.9 | async-start | bytes 2097152 | tf_op jit(solution)/shard_map/all_to_all | solution.py:15
  325.5 2.8 copy-start
where the time goes:
time: 387 us; the launch traced here: 386 us
  blocking collectives  170 us (44%)
  waiting for transfers between devices  126 us (33%)
  starting transfers between devices  42.7 us (11%)
  matrix products  20.6 us (5%)
  local copies, waits for them, and re-layouts  18.4 us (5%)
  other arithmetic  8.24 us (2%)
    all_to_all x3, blocking collectives, copy_for_each(): lax.all_to_all(jnp.broadcast_to(x[None], (count, *x.shape)), axis, 0, 0,...  85.4 us
    all_to_all x2, blocking collectives, summed_on_arrival(): lax.all_to_all(tiles, axis, split_axis=0, concat_axis=0, tiled=True)  84.1 us
    all_to_all x2, waiting for transfers between devices, summed_on_arrival(): lax.all_to_all(tiles, axis, split_axis=0, concat_axis=0, tiled=True)  72.9 us
    all_to_all x3, waiting for transfers between devices, copy_for_each(): lax.all_to_all(jnp.broadcast_to(x[None], (count, *x.shape)), axis, 0, 0,...  52.8 us
    all_to_all x2, starting transfers between devices, summed_on_arrival(): lax.all_to_all(tiles, axis, split_axis=0, concat_axis=0, tiled=True)  27.9 us
    all_to_all x3, starting transfers between devices, copy_for_each(): lax.all_to_all(jnp.broadcast_to(x[None], (count, *x.shape)), axis, 0, 0,...  14.8 us
    dot_general x10, matrix products, shards(): jnp.dot(normed, matrix, preferred_element_type=jnp.float32)  10.7 us
  transfers between devices with their start and end apart: 5, of which 5 were waited for; matrix products, arithmetic and copies ran while one was open for 2% of the time, Pallas kernels for 0%

commit v1 on v0

v1 whole, which is shorter than its diff:
```python
import functools

import jax
import jax.numpy as jnp
from jax import lax
from jax.experimental import pallas as pl
from jax.experimental.pallas import tpu as pltpu
from jax.sharding import PartitionSpec as P

LAYERS = 2
EPS = 1e-06
TAU = 16.0
BF = jnp.bfloat16
F32 = jnp.float32
VMEM_LIMIT = 56 * 1024 * 1024
ROUNDS = 4
SIDE = 128


def dot(a, b):
    return jnp.dot(a, b, preferred_element_type=F32)


def params(*semantics):
    return pltpu.CompilerParams(vmem_limit_bytes=VMEM_LIMIT, dimension_semantics=semantics or None)


def whole(shape):
    return pl.BlockSpec(shape, lambda *_: (0,) * len(shape))


def project(x, gain_ref, w_refs, a_ref, b_ref, lens_col):
    xf = x.astype(F32)
    scaled = jnp.clip(xf * gain_ref[...].astype(F32), -1e30, 1e30).astype(BF)
    wq, wk, wv, wr, wf = w_refs
    at = 0
    for w in (wq, wk, wv):
        a_ref[0, :, at : at + w.shape[-1]] = dot(scaled, w[0]).astype(BF)
        at += w.shape[-1]
    at = 0
    for w in (wr, wf):
        b_ref[0, :, at : at + w.shape[-1]] = dot(scaled, w[0]).astype(BF)
        at += w.shape[-1]
    squares = jnp.sum(xf * xf, axis=1, keepdims=True)
    high = squares.astype(BF).astype(F32)
    low = jnp.where(jnp.abs(high) < 3.0e38, squares - high, 0.0)
    lane = lax.broadcasted_iota(jnp.int32, (x.shape[0], SIDE), 1)
    side = jnp.where(lane == 0, high, jnp.where(lane == 1, low, 0.0))
    if lens_col is not None:
        side = jnp.where(lane == 2, lens_col, side)
    b_ref[0, :, at : at + SIDE] = side.astype(BF)


def project_first(local_seqs, meta, lens, x_ref, gain_ref, wq, wk, wv, wr, wf, a_ref, b_ref):
    rows = x_ref.shape[0]
    row = lax.broadcasted_iota(jnp.int32, (rows, SIDE), 0) - meta[9] * local_seqs
    lens_col = jnp.zeros((rows, SIDE), F32)
    for s in range(local_seqs):
        lens_col = jnp.where(row == s, lens[s].astype(F32), lens_col)
    project(x_ref[...], gain_ref, (wq, wk, wv, wr, wf), a_ref, b_ref, lens_col)


def piece_ids(meta, rows, tp, offset, sign):
    span = rows // ROUNDS
    lane = lax.broadcasted_iota(jnp.int32, (rows, rows), 1)
    block = lax.rem(meta[8] + offset + sign * ROUNDS * (lane // span) + 2 * tp, tp)
    return (block * span + lax.rem(lane, span)).astype(F32)


def expand(meta, tp, where_row, pieces):
    own, plus, minus, far_a, far_b = pieces
    rows = own.shape[0]
    half = far_a.shape[1]
    place = jnp.transpose(jnp.broadcast_to(where_row, (rows, where_row.shape[1])))
    at = jnp.broadcast_to(place[:, :1], (place.shape[0], rows))

    def pick(offset, piece):
        chosen = (at == piece_ids(meta, rows, tp, offset, -1)).astype(F32).astype(BF)
        return dot(chosen, piece)

    near = pick(0, own[...]) + pick(1, plus[...]) + pick(-1, minus[...])
    left = near[:, :half] + pick(2, far_a[...])
    right = near[:, half:] + pick(-2, far_b[...])
    return left, right, place


def project_next(tp, first, meta, where_ref, own, plus, minus, far_a, far_b, gain_ref, wq, wk, wv, wr, wf, a_ref, b_ref):
    owner = meta[first + pl.program_id(0)]
    left, right, _ = expand(meta, tp, where_ref[pl.ds(owner, 1), :], (own, plus, minus, far_a, far_b))
    x = jnp.concatenate([left, right], axis=1)
    project(x, gain_ref, (wq, wk, wv, wr, wf), a_ref, b_ref, None)


def finish(tp, meta, where_ref, own, plus, minus, far_a, far_b, x_ref, out_ref):
    left, right, place = expand(meta, tp, where_ref[pl.ds(pl.program_id(0), 1), :], (own, plus, minus, far_a, far_b))
    half = left.shape[1]
    dead = place[:, :1] < 0
    x = x_ref[...].astype(F32)
    out_ref[:, :half] = jnp.where(dead, x[:, :half], left).astype(BF)
    out_ref[:, half:] = jnp.where(dead, x[:, half:], right).astype(BF)


def weight_spec(layer, w):
    return pl.BlockSpec((1, w.shape[1], w.shape[2]), lambda i, *_: (layer, 0, 0))


def call_project_first(layer, first, meta, lens, x, gain, weights, blocks):
    rows, width = x.shape[0] // (2 * blocks), x.shape[1]
    a_cols = sum(w.shape[2] for w in weights[:3])
    b_cols = sum(w.shape[2] for w in weights[3:]) + SIDE
    return pl.pallas_call(
        functools.partial(project_first, lens.shape[0]),
        grid_spec=pltpu.PrefetchScalarGridSpec(
            num_scalar_prefetch=2,
            grid=(blocks,),
            in_specs=[
                pl.BlockSpec((rows, width), lambda i, meta, lens: (meta[first + i], 0)),
                whole((1, width)),
                *(weight_spec(layer, w) for w in weights),
            ],
            out_specs=[
                pl.BlockSpec((1, rows, a_cols), lambda i, *_: (i, 0, 0)),
                pl.BlockSpec((1, rows, b_cols), lambda i, *_: (i, 0, 0)),
            ],
        ),
        out_shape=[
            jax.ShapeDtypeStruct((blocks, rows, a_cols), BF),
            jax.ShapeDtypeStruct((blocks, rows, b_cols), BF),
        ],
        compiler_params=params("arbitrary"),
        name="project_first",
    )(meta, lens, x, gain[layer : layer + 1], *weights)


def piece_specs(pieces):
    return [whole(p.shape) for p in pieces]


def call_project_next(layer, first, tp, meta, where, pieces, gain, weights, blocks):
    rows, width = where.shape[1], gain.shape[1]
    a_cols = sum(w.shape[2] for w in weights[:3])
    b_cols = sum(w.shape[2] for w in weights[3:]) + SIDE
    return pl.pallas_call(
        functools.partial(project_next, tp, first),
        grid_spec=pltpu.PrefetchScalarGridSpec(
            num_scalar_prefetch=1,
            grid=(blocks,),
            in_specs=[
                whole(where.shape),
                *piece_specs(pieces),
                whole((1, width)),
                *(weight_spec(layer, w) for w in weights),
            ],
            out_specs=[
                pl.BlockSpec((1, rows, a_cols), lambda i, *_: (i, 0, 0)),
                pl.BlockSpec((1, rows, b_cols), lambda i, *_: (i, 0, 0)),
            ],
        ),
        out_shape=[
            jax.ShapeDtypeStruct((blocks, rows, a_cols), BF),
            jax.ShapeDtypeStruct((blocks, rows, b_cols), BF),
        ],
        compiler_params=params("arbitrary"),
        name="project_next",
    )(meta, where, *pieces, gain[layer : layer + 1], *weights)


def call_finish(tp, meta, where, pieces, x):
    owners, rows = where.shape
    return pl.pallas_call(
        functools.partial(finish, tp),
        grid_spec=pltpu.PrefetchScalarGridSpec(
            num_scalar_prefetch=1,
            grid=(owners,),
            in_specs=[
                whole(where.shape),
                *piece_specs(pieces),
                pl.BlockSpec((rows, x.shape[1]), lambda i, *_: (i, 0)),
            ],
            out_specs=pl.BlockSpec((rows, x.shape[1]), lambda i, *_: (i, 0)),
        ),
        out_shape=jax.ShapeDtypeStruct(x.shape, BF),
        compiler_params=params("arbitrary"),
        name="finish",
    )(meta, where, *pieces, x)


def recur(layer, full_width, with_plan, steps, lens, *refs):
    (ma, mb, ca, cb, ra, rb, ra2, rb2, shift_ref, extra_ref, hs_ref, state_hbm), rest = refs[:12], refs[12:]
    if with_plan:
        g_ref, wk_ref, v_ref, end_ref, where_ref, state, sem = rest
    else:
        g_ref, wk_ref, v_ref, end_ref, state, sem = rest
    load = pltpu.make_async_copy(state_hbm.at[layer], state, sem)
    load.start()
    seqs, key_dim, value_dim = state.shape
    rows = seqs * steps
    sum_a = (ma[0].astype(F32) + ca[0].astype(F32)) + (ra[0].astype(F32) + ra2[...].astype(F32))
    sum_b = (mb[0].astype(F32) + cb[0].astype(F32)) + (rb[0].astype(F32) + rb2[...].astype(F32))
    at = value_dim + key_dim
    side = sum_b[:, at : at + SIDE]
    squares = side[:, 0:1] + side[:, 1:2]
    rms = lax.rsqrt(squares / full_width + EPS)
    q = sum_a[:, :key_dim] * (rms * key_dim ** (-0.5))
    k = sum_a[:, key_dim : 2 * key_dim] * rms
    v = sum_a[:, 2 * key_dim :] * rms
    r = sum_b[:, :value_dim] * rms
    f = sum_b[:, value_dim:at] * rms

    row = lax.broadcasted_iota(jnp.int32, (rows, key_dim), 0)
    own_len = jnp.zeros((rows, key_dim), jnp.int32)
    for s in range(seqs):
        own_len = jnp.where(row // steps == s, lens[s], own_len)
    live = jnp.where(lax.rem(row, steps) < own_len, 1.0, 0.0)
    logits = f + shift_ref[...]
    log_sig = jnp.minimum(logits, 0.0) - jnp.log(1.0 + jnp.exp(-jnp.abs(logits)))
    fade = (log_sig / TAU + extra_ref[...]) * live
    k = k * live

    def by_seq(x):
        return x.reshape(seqs, steps, x.shape[1])

    q3, k3, v3, fade3 = by_seq(q), by_seq(k), by_seq(v), by_seq(fade)
    slot = lax.broadcasted_iota(jnp.int32, (seqs, steps, key_dim), 1)
    total = jnp.zeros_like(fade3)
    for j in range(steps):
        total = total + jnp.where(slot >= j, fade3[:, j : j + 1, :], 0.0)
    out = jnp.zeros_like(v3)
    for j in range(steps):
        apart = jnp.where(slot >= j, total - total[:, j : j + 1, :], -1e30)
        score = jnp.sum(q3 * k3[:, j : j + 1, :] * jnp.exp(apart), axis=-1, keepdims=True)
        out = out + score * v3[:, j : j + 1, :]
    last = total[:, steps - 1 : steps, :]
    wk_ref[...] = (k3 * jnp.exp(last - total)).reshape(rows, key_dim).astype(BF)
    v_ref[...] = v.astype(BF)
    end_ref[...] = jnp.exp(last)
    if with_plan:
        owners = where_ref.shape[0]
        n = side.shape[0]
        lens_all = jnp.where(lax.broadcasted_iota(jnp.int32, side.shape, 1) == 0, side[:, 2:3], side[:, 2:3]).astype(BF)
        seq_of = lax.broadcasted_iota(jnp.int32, (n, owners * rows), 1) // steps
        seq = lax.broadcasted_iota(jnp.int32, (n, owners * rows), 0)
        before = (seq < seq_of).astype(F32).astype(BF)
        same = (seq == seq_of).astype(F32).astype(BF)
        over = (((0,), (0,)), ((), ()))
        start = lax.dot_general(lens_all, before, over, preferred_element_type=F32)[:8]
        length = lax.dot_general(lens_all, same, over, preferred_element_type=F32)[:8]
        t = lax.rem(lax.broadcasted_iota(jnp.int32, start.shape, 1), steps).astype(F32)
        spot = jnp.where(t < length, start + t, -1.0)
        for d in range(owners):
            where_ref[d : d + 1, :] = spot[:1, d * rows : (d + 1) * rows]
    weighted = (q3 * jnp.exp(total)).reshape(rows, key_dim).astype(BF)
    load.wait()
    carried = [
        dot(weighted[s * steps : (s + 1) * steps], state[s].astype(BF)) for s in range(seqs)
    ]
    out = out.reshape(rows, value_dim) + jnp.concatenate(carried, axis=0)
    scale = lax.rsqrt(jnp.mean(out * out, axis=-1, keepdims=True) + EPS)
    silu = r / (1.0 + jnp.exp(-r))
    g_ref[...] = (out * scale * hs_ref[...].astype(F32) * silu * live[:, :1]).astype(BF)


def call_recur(layer, full_width, with_plan, owners, lens, parts, shift, extra, head_scale, state, steps):
    _, seqs, key_dim, value_dim = state.shape
    rows = seqs * steps
    blocked = lambda p: pl.BlockSpec((1, *p.shape[1:]), lambda *_: (0, 0, 0))
    ma, mb, ca, cb, ra, rb, ra2, rb2 = parts
    out_shape = [
        jax.ShapeDtypeStruct((rows, value_dim), BF),
        jax.ShapeDtypeStruct((rows, key_dim), BF),
        jax.ShapeDtypeStruct((rows, value_dim), BF),
        jax.ShapeDtypeStruct((seqs, 1, key_dim), F32),
    ]
    if with_plan:
        out_shape.append(jax.ShapeDtypeStruct((owners, rows), F32))
    return pl.pallas_call(
        functools.partial(recur, layer, full_width, with_plan, steps),
        grid_spec=pltpu.PrefetchScalarGridSpec(
            num_scalar_prefetch=1,
            grid=(1,),
            in_specs=[
                blocked(ma),
                blocked(mb),
                blocked(ca),
                blocked(cb),
                blocked(ra),
                pl.BlockSpec((1, *rb.shape[1:]), lambda *_: (1, 0, 0)),
                whole(ra2.shape),
                whole(rb2.shape),
                whole((1, key_dim)),
                whole((rows, 1)),
                whole((1, value_dim)),
                pl.BlockSpec(memory_space=pl.ANY),
            ],
            out_specs=[whole(o.shape) for o in out_shape],
            scratch_shapes=[pltpu.VMEM((seqs, key_dim, value_dim), F32), pltpu.SemaphoreType.DMA],
        ),
        out_shape=out_shape,
        compiler_params=params("arbitrary"),
        name="recur",
    )(lens, *parts, shift[layer : layer + 1], extra, head_scale[layer : layer + 1], state)


def update(steps, wk_ref, v_ref, end_ref, state_ref, *refs):
    out_ref = refs[-1]
    for s in range(state_ref.shape[1]):
        keys = wk_ref[s * steps : (s + 1) * steps, :]
        values = v_ref[s * steps : (s + 1) * steps, :]
        fresh = lax.dot_general(keys, values, (((0,), (0,)), ((), ())), preferred_element_type=F32)
        end = end_ref[s]
        keep = jnp.transpose(jnp.broadcast_to(end, (end.shape[1], end.shape[1])))[:, :1]
        out_ref[0, s] = keep * state_ref[0, s] + fresh


def call_update(layer, steps, wk, v, end, state, previous):
    layers, seqs, key_dim, value_dim = state.shape
    step_seqs = 4
    block = pl.BlockSpec((1, step_seqs, key_dim, value_dim), lambda i: (layer, i, 0, 0))
    operands = [wk, v, end, state]
    in_specs = [
        pl.BlockSpec((step_seqs * steps, key_dim), lambda i: (i, 0)),
        pl.BlockSpec((step_seqs * steps, value_dim), lambda i: (i, 0)),
        pl.BlockSpec((step_seqs, 1, key_dim), lambda i: (i, 0, 0)),
        block,
    ]
    alias = {}
    if previous is not None:
        operands.append(previous)
        in_specs.append(pl.BlockSpec(memory_space=pl.ANY))
        alias = {4: 0}
    return pl.pallas_call(
        functools.partial(update, steps),
        grid=(seqs // step_seqs,),
        in_specs=in_specs,
        out_specs=block,
        out_shape=jax.ShapeDtypeStruct(state.shape, F32),
        input_output_aliases=alias,
        compiler_params=params("arbitrary"),
        name="update_state",
    )(*operands)


def target_ids(meta, count, tp, span):
    row = lax.broadcasted_iota(jnp.int32, (count, 1), 0)
    group = row // (ROUNDS * span)
    offset = jnp.where(group == ROUNDS - 1, tp - 1, group)
    block = lax.rem(meta[8] + offset + ROUNDS * lax.rem(row // span, ROUNDS), tp)
    return (block * span + lax.rem(row, span)).astype(F32)


def close(tp, meta, where_ref, *refs):
    g_refs, (c_ref, own, plus, minus, far_a, far_b) = refs[:8], refs[8:]
    rows = where_ref.shape[1]
    count = own.shape[0] * ROUNDS
    span = count // tp
    ids = jnp.broadcast_to(target_ids(meta, count, tp, span), (count, rows))
    gathered = jnp.zeros((count, g_refs[0].shape[1]), F32)
    for i, g in enumerate(g_refs):
        chosen = (ids == where_ref[pl.ds(meta[i], 1), :]).astype(F32).astype(BF)
        gathered = gathered + dot(chosen, g[...])
    y = dot(gathered.astype(BF), c_ref[0])
    n, half = own.shape[0], far_a.shape[1]
    own[...] = y[:n]
    plus[...] = y[n : 2 * n].astype(BF)
    far_a[...] = y[2 * n : 3 * n, :half].astype(BF)
    far_b[span:, :] = y[2 * n : 3 * n - span, half:].astype(BF)
    far_b[:span, :] = y[3 * n - span : 3 * n, half:].astype(BF)
    minus[...] = y[3 * n :].astype(BF)


def call_close(layer, tp, meta, where, gs, closing, live_rows):
    width = closing.shape[2]
    n = live_rows // ROUNDS
    out_shape = [
        jax.ShapeDtypeStruct((n, width), F32),
        jax.ShapeDtypeStruct((n, width), BF),
        jax.ShapeDtypeStruct((n, width), BF),
        jax.ShapeDtypeStruct((n, width // 2), BF),
        jax.ShapeDtypeStruct((n, width // 2), BF),
    ]
    return pl.pallas_call(
        functools.partial(close, tp),
        grid_spec=pltpu.PrefetchScalarGridSpec(
            num_scalar_prefetch=1,
            grid=(1,),
            in_specs=[
                whole(where.shape),
                *(whole(g.shape) for g in gs),
                pl.BlockSpec((1, *closing.shape[1:]), lambda *_: (layer, 0, 0)),
            ],
            out_specs=[whole(o.shape) for o in out_shape],
        ),
        out_shape=out_shape,
        compiler_params=params("arbitrary"),
        name="close",
    )(meta, where, *gs, closing)


def own_rows(tp, meta, where_ref, x_ref, out_ref):
    span = out_ref.shape[0]
    rows = where_ref.shape[1]
    ids = (meta[8] * span + lax.broadcasted_iota(jnp.int32, (span, rows), 0)).astype(F32)
    total = jnp.zeros(out_ref.shape, F32)
    for d in range(where_ref.shape[0]):
        chosen = (ids == where_ref[d : d + 1, :]).astype(F32).astype(BF)
        total = total + dot(chosen, x_ref[d * rows : (d + 1) * rows, :])
    out_ref[...] = total.astype(BF)


def call_own_rows(tp, meta, where, x, live_rows):
    out = jax.ShapeDtypeStruct((live_rows // tp, x.shape[1]), BF)
    return pl.pallas_call(
        functools.partial(own_rows, tp),
        grid_spec=pltpu.PrefetchScalarGridSpec(
            num_scalar_prefetch=1,
            grid=(1,),
            in_specs=[whole(where.shape), whole(x.shape)],
            out_specs=whole(out.shape),
        ),
        out_shape=out,
        compiler_params=params("arbitrary"),
        name="own_rows",
    )(meta, where, x)


def to_chip(x, flip):
    n = lax.axis_size("dp")
    return lax.ppermute(x, "dp", [(d, 2 * ((d // 2) ^ flip) + d % 2) for d in range(n)])


def to_core(x):
    n = lax.axis_size("dp")
    return lax.ppermute(x, "dp", [(d, d ^ 1) for d in range(n)])


def along(x, step):
    n = lax.axis_size("tp")
    return lax.ppermute(x, "tp", [(i, (i + step) % n) for i in range(n)])


def dp_sum(send, mine):
    (sa, sb), (ma, mb) = send, mine
    ca, cb = to_core(sa), to_core(sb)
    ra = to_chip(ma[1:3] + ca[1:3], 1)
    rb = to_chip(mb[2:4] + cb[2:4], 3)

    def three(m, c, r):
        return (m.astype(F32) + c.astype(F32) + r.astype(F32)).astype(BF)

    ra2 = to_chip(three(ma[3], ca[3], ra[1]), 3)
    rb2 = to_chip(three(mb[1], cb[1], rb[0]), 1)
    return ma, mb, ca, cb, ra, rb, ra2, rb2


def dp_gather(g):
    near = [g, to_chip(g, 1), to_chip(g, 2), to_chip(g, 3)]
    return near + [to_core(x) for x in near]


def tp_sum(parts, x_own, tp):
    own, plus, minus, far_a, far_b = parts
    far = tp // ROUNDS
    r_p = along(plus, 1)
    r_m = along(minus, -1)
    r_a = along(far_a, 2)
    r_b = along(far_b, -2)
    total = own + r_p.astype(F32) + r_m.astype(F32) + jnp.concatenate([r_a, r_b], axis=1).astype(F32)
    total = total.reshape(ROUNDS, -1, total.shape[1])
    arrived = [along(total[j].astype(BF), ROUNDS * j) for j in range(1, far)]
    mixed = total[0]
    for a in arrived:
        mixed = mixed + a.astype(F32)
    return (x_own.astype(F32) + mixed).astype(BF)


def tp_gather(x, tp):
    far = tp // ROUNDS
    own = jnp.concatenate([x] + [along(x, ROUNDS * j) for j in range(1, far)], axis=0)
    half = own.shape[1] // 2
    plus = along(own, -1)
    minus = along(own, 1)
    far_a = along(own[:, :half], -2)
    far_b = along(own[:, half:], 2)
    return own, plus, minus, far_a, far_b


def shards(
    skip_path_activations,
    novel_lengths_per_sequence,
    input_normalizer_scales,
    question_projector,
    lookup_projector,
    payload_projector,
    emitted_valve_projector,
    keeping_valve_projector,
    keeping_valve_shift,
    additional_dwindle_exponent,
    headwise_normalizer_scales,
    closing_projector,
    earlier_recurrence_grid,
):
    streams, steps, width = skip_path_activations.shape
    dp, tp = lax.axis_size("dp"), lax.axis_size("tp")
    chips = dp // 2
    full_width = width * dp
    live_rows = streams * steps // 2
    x = skip_path_activations.reshape(streams * steps, width)
    lens = novel_lengths_per_sequence
    gain = input_normalizer_scales
    weights = (
        question_projector,
        lookup_projector,
        payload_projector,
        emitted_valve_projector,
        keeping_valve_projector,
    )
    layers, seqs, heads, key_dim, value_dim = earlier_recurrence_grid.shape
    state = earlier_recurrence_grid.reshape(layers, seqs * heads, key_dim, value_dim)
    extra = additional_dwindle_exponent.reshape(seqs * steps, 1)

    me = lax.axis_index("dp")
    slot = lax.iota(jnp.int32, 16)
    owner = 2 * ((me // 2) ^ (slot % chips)) + ((me % 2) ^ ((slot // chips) % 2))
    meta = jnp.where(slot == 8, lax.axis_index("tp"), jnp.where(slot == 9, me, owner)).astype(jnp.int32)

    new_state = None
    where = x_own = pieces = None
    for layer in range(layers):
        if layer == 0:
            run = lambda first: call_project_first(layer, first, meta, lens, x, gain, weights, chips)
        else:
            run = lambda first: call_project_next(layer, first, tp, meta, where, pieces, gain, weights, chips)
        send = run(chips)
        mine = run(0)
        parts = dp_sum(send, mine)
        out = call_recur(
            layer, full_width, layer == 0, dp, lens, parts, keeping_valve_shift, extra,
            headwise_normalizer_scales, state, steps,
        )
        if layer == 0:
            g, wk, v, end, where = out
            x_own = call_own_rows(tp, meta, where, x, live_rows)
        else:
            g, wk, v, end = out
        new_state = call_update(layer, steps, wk, v, end, state, new_state)
        sums = call_close(layer, tp, meta, where, dp_gather(g), closing_projector, live_rows)
        x_own = tp_sum(sums, x_own, tp)
        pieces = tp_gather(x_own, tp)
    stream = call_finish(tp, meta, where, pieces, x)
    return (
        stream.reshape(streams, steps, width),
        new_state.reshape(earlier_recurrence_grid.shape),
    )


def solution(mesh):
    in_specs = (
        P("grp", None, "dp"),
        P(("grp", "dp")),
        P(None, "dp"),
        P(None, "dp", "tp"),
        P(None, "dp", "tp"),
        P(None, "dp", "tp"),
        P(None, "dp", "tp"),
        P(None, "dp", "tp"),
        P(None, "tp"),
        P(("grp", "dp"), None, "tp"),
        P(),
        P(None, "tp", "dp"),
        P(None, ("grp", "dp"), "tp", None, None),
    )
    out_specs = (P("grp", None, "dp"), P(None, ("grp", "dp"), "tp", None, None))
    return jax.shard_map(shards, mesh=mesh, in_specs=in_specs, out_specs=out_specs, check_vma=False)
```

time: 387 us -> 269 us (0.70); the launches traced: 386 us -> 263 us
  blocking collectives: 170 us -> 0 us
  starting transfers between devices: 42.7 us -> 122 us
  waiting for transfers between devices: 126 us -> 62.7 us
  Pallas kernels: 0 us -> 57 us
  matrix products: 20.6 us -> 0 us
  local copies, waits for them, and re-layouts: 18.4 us -> 7.87 us
  other arithmetic: 8.24 us -> 12.3 us
    all_to_all x5 -> x0, blocking collectives: 170 us -> none  [the longest x3 85.4 us: copy_for_each(): lax.all_to_all(jnp.broadcast_to(x[None], (count, *x.shape)), axis, 0, 0,...]
    all_to_all x5 -> x0, waiting for transfers between devices: 126 us -> none  [the longest x2 72.9 us: summed_on_arrival(): lax.all_to_all(tiles, axis, split_axis=0, concat_axis=0, tiled=True)]
    ppermute x0 -> x54, starting transfers between devices: none -> 122 us  [the longest x28 92.6 us: along(): return lax.ppermute(x, 'tp', [(i, (i + step) % n) for i in range(n)])]
    ppermute x0 -> x54, waiting for transfers between devices: none -> 62.7 us  [the longest x28 32.6 us: along(): return lax.ppermute(x, 'tp', [(i, (i + step) % n) for i in range(n)])]
    pallas_call x0 -> x12, Pallas kernels: none -> 57 us  [the longest x2 11.4 us: call_project_next(): pl.pallas_call(functools.partial(project_next, tp, first), grid_spec=pltp...]
    all_to_all x5 -> x0, starting transfers between devices: 42.7 us -> none  [the longest x2 27.9 us: summed_on_arrival(): lax.all_to_all(tiles, axis, split_axis=0, concat_axis=0, tiled=True)]
    dot_general x18 -> x0, matrix products: 20.6 us -> none  [the longest x10 10.7 us: shards(): jnp.dot(normed, matrix, preferred_element_type=jnp.float32)]
    another operation x5 -> x0, local copies, waits for them, and re-layouts: 7.52 us -> none  [the longest x1 6.78 us: shards(): ongoing.reshape(number_of_streams, number_of_iterations, shard_breadth)]
  transfers between devices with their start and end apart: 5 -> 54, of which waited for: 5 -> 26; matrix products, arithmetic and copies ran while one was open for 2% -> 4% of each run, Pallas kernels for 0% -> 8%
where the time goes in v1:
time: 269 us; the launch traced here: 263 us
  starting transfers between devices  122 us (45%)
  waiting for transfers between devices  62.7 us (23%)
  Pallas kernels  57 us (21%)
  other arithmetic  12.3 us (5%)
  local copies, waits for them, and re-layouts  7.87 us (3%)
    ppermute x28, starting transfers between devices, along(): return lax.ppermute(x, 'tp', [(i, (i + step) % n) for i in range(n)])  92.6 us
    ppermute x28, waiting for transfers between devices, along(): return lax.ppermute(x, 'tp', [(i, (i + step) % n) for i in range(n)])  32.6 us
    ppermute x14, waiting for transfers between devices, to_chip(): lax.ppermute(x, 'dp', [(d, 2 * (d // 2 ^ flip) + d % 2) for d in range(n)])  27.7 us
    ppermute x14, starting transfers between devices, to_chip(): lax.ppermute(x, 'dp', [(d, 2 * (d // 2 ^ flip) + d % 2) for d in range(n)])  27.5 us
    pallas_call x2, Pallas kernels, call_project_next(): pl.pallas_call(functools.partial(project_next, tp, first), grid_spec=pltp...  11.4 us
    pallas_call x2, Pallas kernels, call_project_first(): pl.pallas_call(functools.partial(project_first, lens.shape[0]), grid_spec...  9.8 us
    pallas_call x2, Pallas kernels, call_recur(): pl.pallas_call(functools.partial(recur, layer, full_width, with_plan, ste...  9.08 us
    pallas_call x2, Pallas kernels, call_update(): pl.pallas_call(functools.partial(update, steps), grid=(seqs // step_seqs,...  8.93 us
  transfers between devices with their start and end apart: 54, of which 26 were waited for; matrix products, arithmetic and copies ran while one was open for 4% of the time, Pallas kernels for 8%

profile of v1, /device:TPU:40, one launch (start us, length us, event | category | flops | bytes accessed | tf_op | source)
XLA Modules:
  0.0 263.4 jit_solution(6722800302294810195)
XLA Ops:
  0.7 1.4 fusion.23
  2.6 5.0 %project_first.3 = (bf16[4,128,512]{2,1,0:T(8,128)(2,1)}, bf16[4,128,512]{2,1,0:T(8,128)(2,1)}) custom-call(s32[16]{0:T(128)} %compare_select_fusion.3.meta, s32[16]{0:T(128)} %lens.7, bf16[1024,512]{1,0:T(8,128)(2,1)} %bitcast.20, bf16[1,512]{1,0:T(2,128)(2,1)} %get-tuple-element.75.gain_ref, bf16[2,512,128]{2,1,0:T(8,128)(2,1)} %wq.7, ...), custom_call_target="tpu_custom_call" | custom-call | tf_op jit(solution)/shard_map/project_first/pallas_call | solution.py:111
  8.1 4.8 %project_first.2 = (bf16[4,128,512]{2,1,0:T(8,128)(2,1)}, bf16[4,128,512]{2,1,0:T(8,128)(2,1)}) custom-call(s32[16]{0:T(128)} %compare_select_fusion.3.meta, s32[16]{0:T(128)} %lens.7, bf16[1024,512]{1,0:T(8,128)(2,1)} %bitcast.21, bf16[1,512]{1,0:T(2,128)(2,1)} %get-tuple-element.75.gain_ref, bf16[2,512,128]{2,1,0:T(8,128)(2,1)} %wq.7, ...), custom_call_target="tpu_custom_call" | custom-call | tf_op jit(solution)/shard_map/project_first/pallas_call | solution.py:111
  12.9 1.1 slice_add_fusion.2
  14.1 3.3 %collective-permute-start.3 = (bf16[2,128,512]{2,1,0:T(8,128)(2,1)S(1)}, bf16[2,128,512]{2,1,0:T(8,128)(2,1)S(1)}, u32[]{:S(2)}, u32[]{:S(2)}) collective-permute-start(bf16[2,128,512]{2,1,0:T(8,128)(2,1)S(1)} %slice_add_fusion.2), channel_id=1, source_target_pairs={{0,6},{1,7},{2,4},{3,5},{4,2},{5,3},{6,0},{7,1},{8,14},{9,15},{10,... | collective-permute-start | bytes 786440 | tf_op jit(solution)/shard_map/ppermute | solution.py:428
  20.1 3.9 %collective-permute-done.3.refs_5_ = bf16[2,128,512]{2,1,0:T(8,128)(2,1)S(1)} collective-permute-done((bf16[2,128,512]{2,1,0:T(8,128)(2,1)S(1)}, bf16[2,128,512]{2,1,0:T(8,128)(2,1)S(1)}, u32[]{:S(2)}, u32[]{:S(2)}) %collective-permute-start.3) | collective-permute-done | bytes 262176 | tf_op jit(solution)/shard_map/ppermute | solution.py:428
  25.3 1.4 collective-permute-done.2.refs_4_
  27.8 1.6 collective-permute-start.4
  30.1 3.9 %collective-permute-done.4.refs_6_ = bf16[128,512]{1,0:T(8,128)(2,1)S(1)} collective-permute-done((bf16[128,512]{1,0:T(8,128)(2,1)S(1)}, bf16[128,512]{1,0:T(8,128)(2,1)S(1)}, u32[]{:S(2)}, u32[]{:S(2)}) %collective-permute-start.4) | collective-permute-done | bytes 131104 | tf_op jit(solution)/shard_map/ppermute | solution.py:428
  34.7 4.5 %recur.2 = (bf16[128,256]{1,0:T(8,128)(2,1)}, bf16[128,128]{1,0:T(8,128)(2,1)}, bf16[128,256]{1,0:T(8,128)(2,1)}, f32[16,1,128]{2,1,0:T(1,128)}, f32[8,128]{1,0:T(8,128)}) custom-call(s32[16]{0:T(128)} %lens.7, bf16[4,128,512]{2,1,0:T(8,128)(2,1)} %get-tuple-element.29.refs_0_, bf16[4,128,512]{2,1,0:T(8,128)(2,1)} %get-tuple-element.30.refs_1_, ...), custom_call_target="tpu_custom_call" | custom-call | tf_op jit(solution)/shard_map/recur/pallas_call | solution.py:276
  39.4 2.9 %collective-permute-start.7 = (bf16[128,256]{1,0:T(8,128)(2,1)}, bf16[128,256]{1,0:T(8,128)(2,1)S(1)}, u32[]{:S(2)}, u32[]{:S(2)}) collective-permute-start(bf16[128,256]{1,0:T(8,128)(2,1)} %get-tuple-element.34.refs_0_), channel_id=1, source_target_pairs={{0,4},{1,5},{2,6},{3,7},{4,0},{5,1},{6,2},{7,3},{8,12},{9,13},{10,... | collective-permute-start | bytes 196616 | tf_op jit(solution)/shard_map/ppermute | solution.py:428
  42.3 1.8 collective-permute-start.8
  45.5 2.5 collective-permute-done.8.refs_3_
  48.0 1.2 collective-permute-done.12.refs_7_
  49.9 3.7 %close.2 = (f32[128,512]{1,0:T(8,128)}, bf16[128,512]{1,0:T(8,128)(2,1)}, bf16[128,512]{1,0:T(8,128)(2,1)}, bf16[128,256]{1,0:T(8,128)(2,1)}, bf16[128,256]{1,0:T(8,128)(2,1)}) custom-call(s32[16]{0:T(128)} %compare_select_fusion.3.meta, f32[8,128]{1,0:T(8,128)} %get-tuple-element.33.where_ref, bf16[128,256]{1,0:T(8,128)(2,1)} %get-tuple-element.34.refs_0_, ...), custom_call_target="tpu_custom_call" | custom-call | tf_op jit(solution)/shard_map/close/pallas_call | solution.py:381
  53.5 2.8 %collective-permute-start.13 = (bf16[128,512]{1,0:T(8,128)(2,1)}, bf16[128,512]{1,0:T(8,128)(2,1)S(1)}, u32[]{:S(2)}, u32[]{:S(2)}) collective-permute-start(bf16[128,512]{1,0:T(8,128)(2,1)} %get-tuple-element.36), channel_id=1, source_target_pairs={{0,8},{8,16},{16,24},{24,32},{32,40},{40,48},{48,56},{56,64},{64,7... | collective-permute-start | bytes 393224 | tf_op jit(solution)/shard_map/ppermute | solution.py:438
  56.3 20.0 %collective-permute-start.14 = (bf16[128,512]{1,0:T(8,128)(2,1)}, bf16[128,512]{1,0:T(8,128)(2,1)S(1)}, u32[]{:S(2)}, u32[]{:S(2)}) collective-permute-start(bf16[128,512]{1,0:T(8,128)(2,1)} %get-tuple-element.37), channel_id=1, source_target_pairs={{0,120},{8,0},{16,8},{24,16},{32,24},{40,32},{48,40},{56,48},{64,5... | collective-permute-start | bytes 393224 | tf_op jit(solution)/shard_map/ppermute | solution.py:438
  76.3 4.1 %collective-permute-start.16 = (bf16[128,256]{1,0:T(8,128)(2,1)}, bf16[128,256]{1,0:T(8,128)(2,1)S(1)}, u32[]{:S(2)}, u32[]{:S(2)}) collective-permute-start(bf16[128,256]{1,0:T(8,128)(2,1)} %get-tuple-element.39), channel_id=1, source_target_pairs={{0,112},{8,120},{16,0},{24,8},{32,16},{40,24},{48,32},{56,40},{64,... | collective-permute-start | bytes 196616 | tf_op jit(solution)/shard_map/ppermute | solution.py:438
  80.4 3.5 %collective-permute-done.15 = bf16[128,256]{1,0:T(8,128)(2,1)S(1)} collective-permute-done((bf16[128,256]{1,0:T(8,128)(2,1)}, bf16[128,256]{1,0:T(8,128)(2,1)S(1)}, u32[]{:S(2)}, u32[]{:S(2)}) %collective-permute-start.15) | collective-permute-done | bytes 65568 | tf_op jit(solution)/shard_map/ppermute | solution.py:438
  85.1 7.5 %collective-permute-start.18 = (bf16[32,512]{1,0:T(8,128)(2,1)S(1)}, bf16[32,512]{1,0:T(8,128)(2,1)S(1)}, u32[]{:S(2)}, u32[]{:S(2)}) collective-permute-start(bf16[32,512]{1,0:T(8,128)(2,1)S(1)} %get-tuple-element.73), channel_id=1, source_target_pairs={{0,64},{8,72},{16,80},{24,88},{32,96},{40,104},{48,112},{56,120},{... | collective-permute-start | bytes 98312 | tf_op jit(solution)/shard_map/ppermute | solution.py:438
  92.6 1.8 collective-permute-start.19
  94.5 2.8 %own_rows.1 = bf16[32,512]{1,0:T(8,128)(2,1)} custom-call(s32[16]{0:T(128)} %compare_select_fusion.3.meta, f32[8,128]{1,0:T(8,128)} %get-tuple-element.33.where_ref, bf16[1024,512]{1,0:T(8,128)(2,1)} %bitcast.22), custom_call_target="tpu_custom_call" | custom-call | tf_op jit(solution)/shard_map/own_rows/pallas_call | solution.py:412
  97.9 2.7 %collective-permute-done.19 = bf16[32,512]{1,0:T(8,128)(2,1)S(1)} collective-permute-done((bf16[32,512]{1,0:T(8,128)(2,1)S(1)}, bf16[32,512]{1,0:T(8,128)(2,1)S(1)}, u32[]{:S(2)}, u32[]{:S(2)}) %collective-permute-start.19) | collective-permute-done | bytes 32800 | tf_op jit(solution)/shard_map/ppermute | solution.py:438
  101.4 4.0 %collective-permute-start.20 = (bf16[32,512]{1,0:T(8,128)(2,1)S(1)}, bf16[32,512]{1,0:T(8,128)(2,1)S(1)}, u32[]{:S(2)}, u32[]{:S(2)}) collective-permute-start(bf16[32,512]{1,0:T(8,128)(2,1)S(1)} %fusion.11), channel_id=1, source_target_pairs={{0,32},{8,40},{16,48},{24,56},{32,64},{40,72},{48,80},{56,88},{64,... | collective-permute-start | bytes 98312 | tf_op jit(solution)/shard_map/ppermute | solution.py:438
  105.5 4.5 %collective-permute-start.21 = (bf16[32,512]{1,0:T(8,128)(2,1)S(1)}, bf16[32,512]{1,0:T(8,128)(2,1)S(1)}, u32[]{:S(2)}, u32[]{:S(2)}) collective-permute-start(bf16[32,512]{1,0:T(8,128)(2,1)S(1)} %fusion.11), channel_id=1, source_target_pairs={{0,64},{8,72},{16,80},{24,88},{32,96},{40,104},{48,112},{56,120},{... | collective-permute-start | bytes 98312 | tf_op jit(solution)/shard_map/ppermute | solution.py:438
  109.9 2.2 collective-permute-start.22
  112.2 6.0 %collective-permute-done.21 = bf16[32,512]{1,0:T(8,128)(2,1)S(1)} collective-permute-done((bf16[32,512]{1,0:T(8,128)(2,1)S(1)}, bf16[32,512]{1,0:T(8,128)(2,1)S(1)}, u32[]{:S(2)}, u32[]{:S(2)}) %collective-permute-start.21) | collective-permute-done | bytes 32800 | tf_op jit(solution)/shard_map/ppermute | solution.py:438
  118.7 3.0 %collective-permute-start.23 = (bf16[128,512]{1,0:T(8,128)(2,1)S(1)}, bf16[128,512]{1,0:T(8,128)(2,1)S(1)}, u32[]{:S(2)}, u32[]{:S(2)}) collective-permute-start(bf16[128,512]{1,0:T(8,128)(2,1)S(1)} %pad_maximum_fusion.own), channel_id=1, source_target_pairs={{0,120},{8,0},{16,8},{24,16},{32,24},{40,32},{48,40},{56,48},{64,5... | collective-permute-start | bytes 393224 | tf_op jit(solution)/shard_map/ppermute | solution.py:438
  121.7 2.3 collective-permute-start.25
  125.0 2.1 collective-permute-done.25.far_a
  127.1 4.0 %collective-permute-done.26.far_b = bf16[128,256]{1,0:T(8,128)(2,1)S(1)} collective-permute-done((bf16[128,256]{1,0:T(8,128)(2,1)S(1)}, bf16[128,256]{1,0:T(8,128)(2,1)S(1)}, u32[]{:S(2)}, u32[]{:S(2)}) %collective-permute-start.26) | collective-permute-done | bytes 65568 | tf_op jit(solution)/shard_map/ppermute | solution.py:438
  131.9 5.7 %project_next.3 = (bf16[4,128,512]{2,1,0:T(8,128)(2,1)}, bf16[4,128,512]{2,1,0:T(8,128)(2,1)}) custom-call(s32[16]{0:T(128)} %compare_select_fusion.3.meta, f32[8,128]{1,0:T(8,128)} %get-tuple-element.33.where_ref, bf16[128,512]{1,0:T(8,128)(2,1)} %copy-done, bf16[128,512]{1,0:T(8,128)(2,1)} %copy-done.10, bf16[128,512]{1,0:T(8,128)(2,1)} %copy-done.11, ...), custom_call_target="tpu_custom_call" | custom-call | tf_op jit(solution)/shard_map/project_next/pallas_call | solution.py:143
  138.1 5.7 %project_next.2 = (bf16[4,128,512]{2,1,0:T(8,128)(2,1)}, bf16[4,128,512]{2,1,0:T(8,128)(2,1)}) custom-call(s32[16]{0:T(128)} %compare_select_fusion.3.meta, f32[8,128]{1,0:T(8,128)} %get-tuple-element.33.where_ref, bf16[128,512]{1,0:T(8,128)(2,1)} %copy-done, bf16[128,512]{1,0:T(8,128)(2,1)} %copy-done.10, bf16[128,512]{1,0:T(8,128)(2,1)} %copy-done.11, ...), custom_call_target="tpu_custom_call" | custom-call | tf_op jit(solution)/shard_map/project_next/pallas_call | solution.py:143
  143.8 1.2 slice_add_fusion
  144.9 10.7 %collective-permute-start.30 = (bf16[2,128,512]{2,1,0:T(8,128)(2,1)S(1)}, bf16[2,128,512]{2,1,0:T(8,128)(2,1)S(1)}, u32[]{:S(2)}, u32[]{:S(2)}) collective-permute-start(bf16[2,128,512]{2,1,0:T(8,128)(2,1)S(1)} %slice_add_fusion), channel_id=1, source_target_pairs={{0,6},{1,7},{2,4},{3,5},{4,2},{5,3},{6,0},{7,1},{8,14},{9,15},{10,... | collective-permute-start | bytes 786440 | tf_op jit(solution)/shard_map/ppermute | solution.py:428
  156.9 6.5 %collective-permute-done.30.refs_5_ = bf16[2,128,512]{2,1,0:T(8,128)(2,1)S(1)} collective-permute-done((bf16[2,128,512]{2,1,0:T(8,128)(2,1)S(1)}, bf16[2,128,512]{2,1,0:T(8,128)(2,1)S(1)}, u32[]{:S(2)}, u32[]{:S(2)}) %collective-permute-start.30) | collective-permute-done | bytes 262176 | tf_op jit(solution)/shard_map/ppermute | solution.py:428
  166.0 1.6 collective-permute-start.31
  167.6 1.9 collective-permute-done.32.refs_7_
  169.5 2.8 %collective-permute-done.31.refs_6_ = bf16[128,512]{1,0:T(8,128)(2,1)S(1)} collective-permute-done((bf16[128,512]{1,0:T(8,128)(2,1)S(1)}, bf16[128,512]{1,0:T(8,128)(2,1)S(1)}, u32[]{:S(2)}, u32[]{:S(2)}) %collective-permute-start.31) | collective-permute-done | bytes 131104 | tf_op jit(solution)/shard_map/ppermute | solution.py:428
  173.0 4.5 %recur.3 = (bf16[128,256]{1,0:T(8,128)(2,1)}, bf16[128,128]{1,0:T(8,128)(2,1)}, bf16[128,256]{1,0:T(8,128)(2,1)}, f32[16,1,128]{2,1,0:T(1,128)}) custom-call(s32[16]{0:T(128)} %lens.7, bf16[4,128,512]{2,1,0:T(8,128)(2,1)} %get-tuple-element.40.refs_0_, bf16[4,128,512]{2,1,0:T(8,128)(2,1)} %get-tuple-element.41.refs_1_, bf16[4,128,512]{2,1,0:T(8,128)(2,1)} %copy-done.4, ...), custom_call_target="tpu_custom_call" | custom-call | tf_op jit(solution)/shard_map/recur/pallas_call | solution.py:276
  178.1 2.5 collective-permute-start.34
  180.5 1.8 collective-permute-start.35
  182.8 1.2 collective-permute-done.34.refs_2_
  184.0 2.2 collective-permute-done.35.refs_3_
  186.3 1.2 collective-permute-done.39.refs_7_
  188.2 3.7 %close.3 = (f32[128,512]{1,0:T(8,128)}, bf16[128,512]{1,0:T(8,128)(2,1)}, bf16[128,512]{1,0:T(8,128)(2,1)}, bf16[128,256]{1,0:T(8,128)(2,1)}, bf16[128,256]{1,0:T(8,128)(2,1)}) custom-call(s32[16]{0:T(128)} %compare_select_fusion.3.meta, f32[8,128]{1,0:T(8,128)} %get-tuple-element.33.where_ref, bf16[128,256]{1,0:T(8,128)(2,1)} %get-tuple-element.44.refs_0_, ...), custom_call_target="tpu_custom_call" | custom-call | tf_op jit(solution)/shard_map/close/pallas_call | solution.py:381
  191.8 1.8 collective-permute-start.40
  193.6 1.4 collective-permute-start.41
  195.2 4.0 %collective-permute-start.43 = (bf16[128,256]{1,0:T(8,128)(2,1)}, bf16[128,256]{1,0:T(8,128)(2,1)S(1)}, u32[]{:S(2)}, u32[]{:S(2)}) collective-permute-start(bf16[128,256]{1,0:T(8,128)(2,1)} %get-tuple-element.49), channel_id=1, source_target_pairs={{0,112},{8,120},{16,0},{24,8},{32,16},{40,24},{48,32},{56,40},{64,... | collective-permute-start | bytes 196616 | tf_op jit(solution)/shard_map/ppermute | solution.py:438
  199.2 2.9 %collective-permute-done.42 = bf16[128,256]{1,0:T(8,128)(2,1)S(1)} collective-permute-done((bf16[128,256]{1,0:T(8,128)(2,1)}, bf16[128,256]{1,0:T(8,128)(2,1)S(1)}, u32[]{:S(2)}, u32[]{:S(2)}) %collective-permute-start.42) | collective-permute-done | bytes 65568 | tf_op jit(solution)/shard_map/ppermute | solution.py:438
  203.7 3.3 %collective-permute-start.44 = (bf16[32,512]{1,0:T(8,128)(2,1)S(1)}, bf16[32,512]{1,0:T(8,128)(2,1)S(1)}, u32[]{:S(2)}, u32[]{:S(2)}) collective-permute-start(bf16[32,512]{1,0:T(8,128)(2,1)S(1)} %get-tuple-element.66), channel_id=1, source_target_pairs={{0,32},{8,40},{16,48},{24,56},{32,64},{40,72},{48,80},{56,88},{64,... | collective-permute-start | bytes 98312 | tf_op jit(solution)/shard_map/ppermute | solution.py:438
  207.0 4.8 %collective-permute-start.45 = (bf16[32,512]{1,0:T(8,128)(2,1)S(1)}, bf16[32,512]{1,0:T(8,128)(2,1)S(1)}, u32[]{:S(2)}, u32[]{:S(2)}) collective-permute-start(bf16[32,512]{1,0:T(8,128)(2,1)S(1)} %get-tuple-element.68), channel_id=1, source_target_pairs={{0,64},{8,72},{16,80},{24,88},{32,96},{40,104},{48,112},{56,120},{... | collective-permute-start | bytes 98312 | tf_op jit(solution)/shard_map/ppermute | solution.py:438
  211.8 3.7 %collective-permute-start.46 = (bf16[32,512]{1,0:T(8,128)(2,1)S(1)}, bf16[32,512]{1,0:T(8,128)(2,1)S(1)}, u32[]{:S(2)}, u32[]{:S(2)}) collective-permute-start(bf16[32,512]{1,0:T(8,128)(2,1)S(1)} %get-tuple-element.67), channel_id=1, source_target_pairs={{0,96},{8,104},{16,112},{24,120},{32,0},{40,8},{48,16},{56,24},{64... | collective-permute-start | bytes 98312 | tf_op jit(solution)/shard_map/ppermute | solution.py:438
  215.4 4.4 %collective-permute-done.45 = bf16[32,512]{1,0:T(8,128)(2,1)S(1)} collective-permute-done((bf16[32,512]{1,0:T(8,128)(2,1)S(1)}, bf16[32,512]{1,0:T(8,128)(2,1)S(1)}, u32[]{:S(2)}, u32[]{:S(2)}) %collective-permute-start.45) | collective-permute-done | bytes 32800 | tf_op jit(solution)/shard_map/ppermute | solution.py:438
  219.8 4.2 %collective-permute-start.47 = (bf16[32,512]{1,0:T(8,128)(2,1)S(1)}, bf16[32,512]{1,0:T(8,128)(2,1)S(1)}, u32[]{:S(2)}, u32[]{:S(2)}) collective-permute-start(bf16[32,512]{1,0:T(8,128)(2,1)S(1)} %fusion.7), channel_id=1, source_target_pairs={{0,32},{8,40},{16,48},{24,56},{32,64},{40,72},{48,80},{56,88},{64,... | collective-permute-start | bytes 98312 | tf_op jit(solution)/shard_map/ppermute | solution.py:438
  224.0 5.9 %collective-permute-start.48 = (bf16[32,512]{1,0:T(8,128)(2,1)S(1)}, bf16[32,512]{1,0:T(8,128)(2,1)S(1)}, u32[]{:S(2)}, u32[]{:S(2)}) collective-permute-start(bf16[32,512]{1,0:T(8,128)(2,1)S(1)} %fusion.7), channel_id=1, source_target_pairs={{0,64},{8,72},{16,80},{24,88},{32,96},{40,104},{48,112},{56,120},{... | collective-permute-start | bytes 98312 | tf_op jit(solution)/shard_map/ppermute | solution.py:438
  229.9 3.2 %collective-permute-start.49 = (bf16[32,512]{1,0:T(8,128)(2,1)S(1)}, bf16[32,512]{1,0:T(8,128)(2,1)S(1)}, u32[]{:S(2)}, u32[]{:S(2)}) collective-permute-start(bf16[32,512]{1,0:T(8,128)(2,1)S(1)} %fusion.7), channel_id=1, source_target_pairs={{0,96},{8,104},{16,112},{24,120},{32,0},{40,8},{48,16},{56,24},{64... | collective-permute-start | bytes 98312 | tf_op jit(solution)/shard_map/ppermute | solution.py:438
  233.2 3.6 %collective-permute-done.48 = bf16[32,512]{1,0:T(8,128)(2,1)S(1)} collective-permute-done((bf16[32,512]{1,0:T(8,128)(2,1)S(1)}, bf16[32,512]{1,0:T(8,128)(2,1)S(1)}, u32[]{:S(2)}, u32[]{:S(2)}) %collective-permute-start.48) | collective-permute-done | bytes 32800 | tf_op jit(solution)/shard_map/ppermute | solution.py:438
  236.8 1.7 collective-permute-done.49
  238.5 3.0 %collective-permute-start.50 = (bf16[128,512]{1,0:T(8,128)(2,1)S(1)}, bf16[128,512]{1,0:T(8,128)(2,1)S(1)}, u32[]{:S(2)}, u32[]{:S(2)}) collective-permute-start(bf16[128,512]{1,0:T(8,128)(2,1)S(1)} %pad_maximum_fusion.1.own), channel_id=1, source_target_pairs={{0,120},{8,0},{16,8},{24,16},{32,24},{40,32},{48,40},{56,48},{64,5... | collective-permute-start | bytes 393224 | tf_op jit(solution)/shard_map/ppermute | solution.py:438
  241.5 3.7 %collective-permute-start.52 = (bf16[128,256]{1,0:T(8,128)(2,1)S(1)}, bf16[128,256]{1,0:T(8,128)(2,1)S(1)}, u32[]{:S(2)}, u32[]{:S(2)}) collective-permute-start(bf16[128,256]{1,0:T(8,128)(2,1)S(1)} %get-tuple-element.65), channel_id=1, source_target_pairs={{0,112},{8,120},{16,0},{24,8},{32,16},{40,24},{48,32},{56,40},{64,... | collective-permute-start | bytes 196616 | tf_op jit(solution)/shard_map/ppermute | solution.py:438
  245.2 4.5 %update_state.2.refs_0_ = f32[2,16,128,256]{3,2,1,0:T(8,128)} custom-call(bf16[128,128]{1,0:T(8,128)(2,1)} %get-tuple-element.53.wk_ref, bf16[128,256]{1,0:T(8,128)(2,1)} %get-tuple-element.54.v_ref, f32[16,1,128]{2,1,0:T(1,128)} %get-tuple-element.55.end_ref, f32[2,16,128,256]{3,2,1,0:T(8,128)} %bitcast.18), custom_call_target="tpu_custom_call" | custom-call | tf_op jit(solution)/shard_map/update_state/pallas_call | solution.py:331
  249.7 4.5 %update_state.3 = f32[2,16,128,256]{3,2,1,0:T(8,128)} custom-call(bf16[128,128]{1,0:T(8,128)(2,1)} %get-tuple-element.50.wk_ref, bf16[128,256]{1,0:T(8,128)(2,1)} %get-tuple-element.51.v_ref, f32[16,1,128]{2,1,0:T(1,128)} %get-tuple-element.52.end_ref, f32[2,16,128,256]{3,2,1,0:T(8,128)} %bitcast.19, ...), custom_call_target="tpu_custom_call", output_to_operand_aliasing={{}: (4, {})} | custom-call | tf_op jit(solution)/shard_map/update_state/pallas_call | solution.py:331
  255.5 7.6 %finish.1 = bf16[1024,512]{1,0:T(8,128)(2,1)} custom-call(s32[16]{0:T(128)} %compare_select_fusion.3.meta, f32[8,128]{1,0:T(8,128)} %get-tuple-element.33.where_ref, bf16[128,512]{1,0:T(8,128)(2,1)} %copy-done.5, bf16[128,512]{1,0:T(8,128)(2,1)} %copy-done.14, bf16[128,512]{1,0:T(8,128)(2,1)} %copy-done.15, bf16[128,256]{1,0:T(8,128)(2,1)} %copy-done.20, ...), custom_call_target="tpu_custom_call" | custom-call | tf_op jit(solution)/shard_map/finish/pallas_call | solution.py:170
  (158 shorter events, 24.6 us)
Async XLA Ops:
  0.6 18.1 %copy-start.37 = (bf16[2,256]{1,0:T(2,128)(2,1)S(1)}, bf16[2,256]{1,0:T(2,128)(2,1)}, u32[]{:S(2)}) copy-start(bf16[2,256]{1,0:T(2,128)(2,1)} %param.23) | copy-start | bytes 3076
  0.6 18.7 %copy-start.36 = (f32[16,8,1]{0,2,1:T(1,128)S(1)}, f32[16,8,1]{0,2,1:T(1,128)}, u32[]{:S(2)}) copy-start(f32[16,8,1]{0,2,1:T(1,128)} %param.22) | copy-start | bytes 1540
  2.6 26.7 %copy-start.38 = (f32[2,128]{1,0:T(2,128)S(1)}, f32[2,128]{1,0:T(2,128)}, u32[]{:S(2)}) copy-start(f32[2,128]{1,0:T(2,128)} %param.21) | copy-start | bytes 3076
  7.6 5.4 %collective-permute-start.1 = (bf16[4,128,512]{2,1,0:T(8,128)(2,1)}, bf16[4,128,512]{2,1,0:T(8,128)(2,1)S(1)}, u32[]{:S(2)}, u32[]{:S(2)}) collective-permute-start(bf16[4,128,512]{2,1,0:T(8,128)(2,1)} %get-tuple-element.32), channel_id=1, source_target_pairs={{0,1},{1,0},{2,3},{3,2},{4,5},{5,4},{6,7},{7,6},{8,9},{9,8},{10,11... | collective-permute-start | bytes 1572872 | tf_op jit(solution)/shard_map/ppermute | solution.py:433
  7.6 9.8 %collective-permute-start = (bf16[4,128,512]{2,1,0:T(8,128)(2,1)}, bf16[4,128,512]{2,1,0:T(8,128)(2,1)S(1)}, u32[]{:S(2)}, u32[]{:S(2)}) collective-permute-start(bf16[4,128,512]{2,1,0:T(8,128)(2,1)} %get-tuple-element.31), channel_id=1, source_target_pairs={{0,1},{1,0},{2,3},{3,2},{4,5},{5,4},{6,7},{7,6},{8,9},{9,8},{10,11... | collective-permute-start | bytes 1572872 | tf_op jit(solution)/shard_map/ppermute | solution.py:433
  12.9 21.1 %copy-start.1 = (bf16[4,128,512]{2,1,0:T(8,128)(2,1)}, bf16[4,128,512]{2,1,0:T(8,128)(2,1)S(1)}, u32[]{:S(2)}) copy-start(bf16[4,128,512]{2,1,0:T(8,128)(2,1)S(1)} %collective-permute-done.1.refs_3_) | copy-start | bytes 1572868
  14.1 9.9 %collective-permute-start.3 = (bf16[2,128,512]{2,1,0:T(8,128)(2,1)S(1)}, bf16[2,128,512]{2,1,0:T(8,128)(2,1)S(1)}, u32[]{:S(2)}, u32[]{:S(2)}) collective-permute-start(bf16[2,128,512]{2,1,0:T(8,128)(2,1)S(1)} %slice_add_fusion.2), channel_id=1, source_target_pairs={{0,6},{1,7},{2,4},{3,5},{4,2},{5,3},{6,0},{7,1},{8,14},{9,15},{10,... | collective-permute-start | bytes 786440 | tf_op jit(solution)/shard_map/ppermute | solution.py:428
  17.4 16.7 %copy-start.3 = (bf16[4,128,512]{2,1,0:T(8,128)(2,1)}, bf16[4,128,512]{2,1,0:T(8,128)(2,1)S(1)}, u32[]{:S(2)}) copy-start(bf16[4,128,512]{2,1,0:T(8,128)(2,1)S(1)} %collective-permute-done.refs_2_) | copy-start | bytes 1572868
  18.5 8.2 %collective-permute-start.2 = (bf16[2,128,512]{2,1,0:T(8,128)(2,1)S(1)}, bf16[2,128,512]{2,1,0:T(8,128)(2,1)S(1)}, u32[]{:S(2)}, u32[]{:S(2)}) collective-permute-start(bf16[2,128,512]{2,1,0:T(8,128)(2,1)S(1)} %slice_add_fusion.3), channel_id=1, source_target_pairs={{0,2},{1,3},{2,0},{3,1},{4,6},{5,7},{6,4},{7,5},{8,10},{9,11},{10,... | collective-permute-start | bytes 786440 | tf_op jit(solution)/shard_map/ppermute | solution.py:428
  24.0 10.1 %copy-start.6 = (bf16[2,128,512]{2,1,0:T(8,128)(2,1)}, bf16[2,128,512]{2,1,0:T(8,128)(2,1)S(1)}, u32[]{:S(2)}) copy-start(bf16[2,128,512]{2,1,0:T(8,128)(2,1)S(1)} %collective-permute-done.3.refs_5_) | copy-start | bytes 786436
  25.0 5.1 %collective-permute-start.5 = (bf16[128,512]{1,0:T(8,128)(2,1)S(1)}, bf16[128,512]{1,0:T(8,128)(2,1)S(1)}, u32[]{:S(2)}, u32[]{:S(2)}) collective-permute-start(bf16[128,512]{1,0:T(8,128)(2,1)S(1)} %fusion.1), channel_id=1, source_target_pairs={{0,2},{1,3},{2,0},{3,1},{4,6},{5,7},{6,4},{7,5},{8,10},{9,11},{10,... | collective-permute-start | bytes 393224 | tf_op jit(solution)/shard_map/ppermute | solution.py:428
  27.8 6.3 %collective-permute-start.4 = (bf16[128,512]{1,0:T(8,128)(2,1)S(1)}, bf16[128,512]{1,0:T(8,128)(2,1)S(1)}, u32[]{:S(2)}, u32[]{:S(2)}) collective-permute-start(bf16[128,512]{1,0:T(8,128)(2,1)S(1)} %fusion), channel_id=1, source_target_pairs={{0,6},{1,7},{2,4},{3,5},{4,2},{5,3},{6,0},{7,1},{8,14},{9,15},{10,... | collective-permute-start | bytes 393224 | tf_op jit(solution)/shard_map/ppermute | solution.py:428
  39.3 4.8 %collective-permute-start.6 = (bf16[128,256]{1,0:T(8,128)(2,1)}, bf16[128,256]{1,0:T(8,128)(2,1)S(1)}, u32[]{:S(2)}, u32[]{:S(2)}) collective-permute-start(bf16[128,256]{1,0:T(8,128)(2,1)} %get-tuple-element.34.refs_0_), channel_id=1, source_target_pairs={{0,2},{1,3},{2,0},{3,1},{4,6},{5,7},{6,4},{7,5},{8,10},{9,11},{10,... | collective-permute-start | bytes 196616 | tf_op jit(solution)/shard_map/ppermute | solution.py:428
  39.4 6.1 %collective-permute-start.7 = (bf16[128,256]{1,0:T(8,128)(2,1)}, bf16[128,256]{1,0:T(8,128)(2,1)S(1)}, u32[]{:S(2)}, u32[]{:S(2)}) collective-permute-start(bf16[128,256]{1,0:T(8,128)(2,1)} %get-tuple-element.34.refs_0_), channel_id=1, source_target_pairs={{0,4},{1,5},{2,6},{3,7},{4,0},{5,1},{6,2},{7,3},{8,12},{9,13},{10,... | collective-permute-start | bytes 196616 | tf_op jit(solution)/shard_map/ppermute | solution.py:428
  42.3 5.7 %collective-permute-start.8 = (bf16[128,256]{1,0:T(8,128)(2,1)}, bf16[128,256]{1,0:T(8,128)(2,1)S(1)}, u32[]{:S(2)}, u32[]{:S(2)}) collective-permute-start(bf16[128,256]{1,0:T(8,128)(2,1)} %get-tuple-element.34.refs_0_), channel_id=1, source_target_pairs={{0,6},{1,7},{2,4},{3,5},{4,2},{5,3},{6,0},{7,1},{8,14},{9,15},{10,... | collective-permute-start | bytes 196616 | tf_op jit(solution)/shard_map/ppermute | solution.py:428
  44.1 3.9 %collective-permute-start.9 = (bf16[128,256]{1,0:T(8,128)(2,1)}, bf16[128,256]{1,0:T(8,128)(2,1)S(1)}, u32[]{:S(2)}, u32[]{:S(2)}) collective-permute-start(bf16[128,256]{1,0:T(8,128)(2,1)} %get-tuple-element.34.refs_0_), channel_id=1, source_target_pairs={{0,1},{1,0},{2,3},{3,2},{4,5},{5,4},{6,7},{7,6},{8,9},{9,8},{10,11... | collective-permute-start | bytes 196616 | tf_op jit(solution)/shard_map/ppermute | solution.py:433
  44.1 3.9 %collective-permute-start.10 = (bf16[128,256]{1,0:T(8,128)(2,1)S(1)}, bf16[128,256]{1,0:T(8,128)(2,1)S(1)}, u32[]{:S(2)}, u32[]{:S(2)}) collective-permute-start(bf16[128,256]{1,0:T(8,128)(2,1)S(1)} %collective-permute-done.6.refs_1_), channel_id=1, source_target_pairs={{0,1},{1,0},{2,3},{3,2},{4,5},{5,4},{6,7},{7,6},{8,9},{9,8},{10,11... | collective-permute-start | bytes 196616 | tf_op jit(solution)/shard_map/ppermute | solution.py:433
  45.5 2.5 collective-permute-start.11
  48.0 1.3 collective-permute-start.12
  53.5 30.4 %collective-permute-start.13 = (bf16[128,512]{1,0:T(8,128)(2,1)}, bf16[128,512]{1,0:T(8,128)(2,1)S(1)}, u32[]{:S(2)}, u32[]{:S(2)}) collective-permute-start(bf16[128,512]{1,0:T(8,128)(2,1)} %get-tuple-element.36), channel_id=1, source_target_pairs={{0,8},{8,16},{16,24},{24,32},{32,40},{40,48},{48,56},{56,64},{64,7... | collective-permute-start | bytes 393224 | tf_op jit(solution)/shard_map/ppermute | solution.py:438
  56.3 27.6 %collective-permute-start.14 = (bf16[128,512]{1,0:T(8,128)(2,1)}, bf16[128,512]{1,0:T(8,128)(2,1)S(1)}, u32[]{:S(2)}, u32[]{:S(2)}) collective-permute-start(bf16[128,512]{1,0:T(8,128)(2,1)} %get-tuple-element.37), channel_id=1, source_target_pairs={{0,120},{8,0},{16,8},{24,16},{32,24},{40,32},{48,40},{56,48},{64,5... | collective-permute-start | bytes 393224 | tf_op jit(solution)/shard_map/ppermute | solution.py:438
  76.3 7.6 %collective-permute-start.15 = (bf16[128,256]{1,0:T(8,128)(2,1)}, bf16[128,256]{1,0:T(8,128)(2,1)S(1)}, u32[]{:S(2)}, u32[]{:S(2)}) collective-permute-start(bf16[128,256]{1,0:T(8,128)(2,1)} %get-tuple-element.38), channel_id=1, source_target_pairs={{0,16},{8,24},{16,32},{24,40},{32,48},{40,56},{48,64},{56,72},{64,... | collective-permute-start | bytes 196616 | tf_op jit(solution)/shard_map/ppermute | solution.py:438
  76.3 7.6 %collective-permute-start.16 = (bf16[128,256]{1,0:T(8,128)(2,1)}, bf16[128,256]{1,0:T(8,128)(2,1)S(1)}, u32[]{:S(2)}, u32[]{:S(2)}) collective-permute-start(bf16[128,256]{1,0:T(8,128)(2,1)} %get-tuple-element.39), channel_id=1, source_target_pairs={{0,112},{8,120},{16,0},{24,8},{32,16},{40,24},{48,32},{56,40},{64,... | collective-permute-start | bytes 196616 | tf_op jit(solution)/shard_map/ppermute | solution.py:438
  85.0 12.2 %collective-permute-start.17 = (bf16[32,512]{1,0:T(8,128)(2,1)S(1)}, bf16[32,512]{1,0:T(8,128)(2,1)S(1)}, u32[]{:S(2)}, u32[]{:S(2)}) collective-permute-start(bf16[32,512]{1,0:T(8,128)(2,1)S(1)} %get-tuple-element.71), channel_id=1, source_target_pairs={{0,32},{8,40},{16,48},{24,56},{32,64},{40,72},{48,80},{56,88},{64,... | collective-permute-start | bytes 98312 | tf_op jit(solution)/shard_map/ppermute | solution.py:438
  85.1 12.8 %collective-permute-start.18 = (bf16[32,512]{1,0:T(8,128)(2,1)S(1)}, bf16[32,512]{1,0:T(8,128)(2,1)S(1)}, u32[]{:S(2)}, u32[]{:S(2)}) collective-permute-start(bf16[32,512]{1,0:T(8,128)(2,1)S(1)} %get-tuple-element.73), channel_id=1, source_target_pairs={{0,64},{8,72},{16,80},{24,88},{32,96},{40,104},{48,112},{56,120},{... | collective-permute-start | bytes 98312 | tf_op jit(solution)/shard_map/ppermute | solution.py:438
  92.6 8.0 %collective-permute-start.19 = (bf16[32,512]{1,0:T(8,128)(2,1)S(1)}, bf16[32,512]{1,0:T(8,128)(2,1)S(1)}, u32[]{:S(2)}, u32[]{:S(2)}) collective-permute-start(bf16[32,512]{1,0:T(8,128)(2,1)S(1)} %get-tuple-element.72), channel_id=1, source_target_pairs={{0,96},{8,104},{16,112},{24,120},{32,0},{40,8},{48,16},{56,24},{64... | collective-permute-start | bytes 98312 | tf_op jit(solution)/shard_map/ppermute | solution.py:438
  101.4 10.7 %collective-permute-start.20 = (bf16[32,512]{1,0:T(8,128)(2,1)S(1)}, bf16[32,512]{1,0:T(8,128)(2,1)S(1)}, u32[]{:S(2)}, u32[]{:S(2)}) collective-permute-start(bf16[32,512]{1,0:T(8,128)(2,1)S(1)} %fusion.11), channel_id=1, source_target_pairs={{0,32},{8,40},{16,48},{24,56},{32,64},{40,72},{48,80},{56,88},{64,... | collective-permute-start | bytes 98312 | tf_op jit(solution)/shard_map/ppermute | solution.py:438
  105.5 12.6 %collective-permute-start.21 = (bf16[32,512]{1,0:T(8,128)(2,1)S(1)}, bf16[32,512]{1,0:T(8,128)(2,1)S(1)}, u32[]{:S(2)}, u32[]{:S(2)}) collective-permute-start(bf16[32,512]{1,0:T(8,128)(2,1)S(1)} %fusion.11), channel_id=1, source_target_pairs={{0,64},{8,72},{16,80},{24,88},{32,96},{40,104},{48,112},{56,120},{... | collective-permute-start | bytes 98312 | tf_op jit(solution)/shard_map/ppermute | solution.py:438
  109.9 8.7 %collective-permute-start.22 = (bf16[32,512]{1,0:T(8,128)(2,1)S(1)}, bf16[32,512]{1,0:T(8,128)(2,1)S(1)}, u32[]{:S(2)}, u32[]{:S(2)}) collective-permute-start(bf16[32,512]{1,0:T(8,128)(2,1)S(1)} %fusion.11), channel_id=1, source_target_pairs={{0,96},{8,104},{16,112},{24,120},{32,0},{40,8},{48,16},{56,24},{64... | collective-permute-start | bytes 98312 | tf_op jit(solution)/shard_map/ppermute | solution.py:438
  118.7 12.5 %copy-start = (bf16[128,512]{1,0:T(8,128)(2,1)}, bf16[128,512]{1,0:T(8,128)(2,1)S(1)}, u32[]{:S(2)}) copy-start(bf16[128,512]{1,0:T(8,128)(2,1)S(1)} %pad_maximum_fusion.own) | copy-start | bytes 393220
  118.7 12.5 %collective-permute-start.23 = (bf16[128,512]{1,0:T(8,128)(2,1)S(1)}, bf16[128,512]{1,0:T(8,128)(2,1)S(1)}, u32[]{:S(2)}, u32[]{:S(2)}) collective-permute-start(bf16[128,512]{1,0:T(8,128)(2,1)S(1)} %pad_maximum_fusion.own), channel_id=1, source_target_pairs={{0,120},{8,0},{16,8},{24,16},{32,24},{40,32},{48,40},{56,48},{64,5... | collective-permute-start | bytes 393224 | tf_op jit(solution)/shard_map/ppermute | solution.py:438
  121.7 9.5 %collective-permute-start.24 = (bf16[128,512]{1,0:T(8,128)(2,1)S(1)}, bf16[128,512]{1,0:T(8,128)(2,1)S(1)}, u32[]{:S(2)}, u32[]{:S(2)}) collective-permute-start(bf16[128,512]{1,0:T(8,128)(2,1)S(1)} %pad_maximum_fusion.own), channel_id=1, source_target_pairs={{0,8},{8,16},{16,24},{24,32},{32,40},{40,48},{48,56},{56,64},{64,7... | collective-permute-start | bytes 393224 | tf_op jit(solution)/shard_map/ppermute | solution.py:438
  121.7 5.4 %collective-permute-start.25 = (bf16[128,256]{1,0:T(8,128)(2,1)S(1)}, bf16[128,256]{1,0:T(8,128)(2,1)S(1)}, u32[]{:S(2)}, u32[]{:S(2)}) collective-permute-start(bf16[128,256]{1,0:T(8,128)(2,1)S(1)} %get-tuple-element.70), channel_id=1, source_target_pairs={{0,112},{8,120},{16,0},{24,8},{32,16},{40,24},{48,32},{56,40},{64,... | collective-permute-start | bytes 196616 | tf_op jit(solution)/shard_map/ppermute | solution.py:438
  124.0 7.2 %collective-permute-start.26 = (bf16[128,256]{1,0:T(8,128)(2,1)S(1)}, bf16[128,256]{1,0:T(8,128)(2,1)S(1)}, u32[]{:S(2)}, u32[]{:S(2)}) collective-permute-start(bf16[128,256]{1,0:T(8,128)(2,1)S(1)} %get-tuple-element.69), channel_id=1, source_target_pairs={{0,16},{8,24},{16,32},{24,40},{32,48},{40,56},{48,64},{56,72},{64,... | collective-permute-start | bytes 196616 | tf_op jit(solution)/shard_map/ppermute | solution.py:438
  137.6 6.2 %collective-permute-start.28 = (bf16[4,128,512]{2,1,0:T(8,128)(2,1)}, bf16[4,128,512]{2,1,0:T(8,128)(2,1)S(1)}, u32[]{:S(2)}, u32[]{:S(2)}) collective-permute-start(bf16[4,128,512]{2,1,0:T(8,128)(2,1)} %get-tuple-element.43), channel_id=1, source_target_pairs={{0,1},{1,0},{2,3},{3,2},{4,5},{5,4},{6,7},{7,6},{8,9},{9,8},{10,11... | collective-permute-start | bytes 1572872 | tf_op jit(solution)/shard_map/ppermute | solution.py:433
  137.6 18.1 %collective-permute-start.27 = (bf16[4,128,512]{2,1,0:T(8,128)(2,1)}, bf16[4,128,512]{2,1,0:T(8,128)(2,1)S(1)}, u32[]{:S(2)}, u32[]{:S(2)}) collective-permute-start(bf16[4,128,512]{2,1,0:T(8,128)(2,1)} %get-tuple-element.42), channel_id=1, source_target_pairs={{0,1},{1,0},{2,3},{3,2},{4,5},{5,4},{6,7},{7,6},{8,9},{9,8},{10,11... | collective-permute-start | bytes 1572872 | tf_op jit(solution)/shard_map/ppermute | solution.py:433
  143.7 28.6 %copy-start.2 = (bf16[4,128,512]{2,1,0:T(8,128)(2,1)}, bf16[4,128,512]{2,1,0:T(8,128)(2,1)S(1)}, u32[]{:S(2)}) copy-start(bf16[4,128,512]{2,1,0:T(8,128)(2,1)S(1)} %collective-permute-done.28.refs_3_) | copy-start | bytes 1572868
  144.9 18.5 %collective-permute-start.30 = (bf16[2,128,512]{2,1,0:T(8,128)(2,1)S(1)}, bf16[2,128,512]{2,1,0:T(8,128)(2,1)S(1)}, u32[]{:S(2)}, u32[]{:S(2)}) collective-permute-start(bf16[2,128,512]{2,1,0:T(8,128)(2,1)S(1)} %slice_add_fusion), channel_id=1, source_target_pairs={{0,6},{1,7},{2,4},{3,5},{4,2},{5,3},{6,0},{7,1},{8,14},{9,15},{10,... | collective-permute-start | bytes 786440 | tf_op jit(solution)/shard_map/ppermute | solution.py:428
  155.6 16.7 %copy-start.4 = (bf16[4,128,512]{2,1,0:T(8,128)(2,1)}, bf16[4,128,512]{2,1,0:T(8,128)(2,1)S(1)}, u32[]{:S(2)}) copy-start(bf16[4,128,512]{2,1,0:T(8,128)(2,1)S(1)} %collective-permute-done.27.refs_2_) | copy-start | bytes 1572868
  156.8 8.2 %collective-permute-start.29 = (bf16[2,128,512]{2,1,0:T(8,128)(2,1)S(1)}, bf16[2,128,512]{2,1,0:T(8,128)(2,1)S(1)}, u32[]{:S(2)}, u32[]{:S(2)}) collective-permute-start(bf16[2,128,512]{2,1,0:T(8,128)(2,1)S(1)} %slice_add_fusion.1), channel_id=1, source_target_pairs={{0,2},{1,3},{2,0},{3,1},{4,6},{5,7},{6,4},{7,5},{8,10},{9,11},{10,... | collective-permute-start | bytes 786440 | tf_op jit(solution)/shard_map/ppermute | solution.py:428
  164.4 5.1 %collective-permute-start.32 = (bf16[128,512]{1,0:T(8,128)(2,1)S(1)}, bf16[128,512]{1,0:T(8,128)(2,1)S(1)}, u32[]{:S(2)}, u32[]{:S(2)}) collective-permute-start(bf16[128,512]{1,0:T(8,128)(2,1)S(1)} %fusion.3), channel_id=1, source_target_pairs={{0,2},{1,3},{2,0},{3,1},{4,6},{5,7},{6,4},{7,5},{8,10},{9,11},{10,... | collective-permute-start | bytes 393224 | tf_op jit(solution)/shard_map/ppermute | solution.py:428
  166.0 6.3 %collective-permute-start.31 = (bf16[128,512]{1,0:T(8,128)(2,1)S(1)}, bf16[128,512]{1,0:T(8,128)(2,1)S(1)}, u32[]{:S(2)}, u32[]{:S(2)}) collective-permute-start(bf16[128,512]{1,0:T(8,128)(2,1)S(1)} %fusion.2), channel_id=1, source_target_pairs={{0,6},{1,7},{2,4},{3,5},{4,2},{5,3},{6,0},{7,1},{8,14},{9,15},{10,... | collective-permute-start | bytes 393224 | tf_op jit(solution)/shard_map/ppermute | solution.py:428
  177.5 4.8 %collective-permute-start.33 = (bf16[128,256]{1,0:T(8,128)(2,1)}, bf16[128,256]{1,0:T(8,128)(2,1)S(1)}, u32[]{:S(2)}, u32[]{:S(2)}) collective-permute-start(bf16[128,256]{1,0:T(8,128)(2,1)} %get-tuple-element.44.refs_0_), channel_id=1, source_target_pairs={{0,2},{1,3},{2,0},{3,1},{4,6},{5,7},{6,4},{7,5},{8,10},{9,11},{10,... | collective-permute-start | bytes 196616 | tf_op jit(solution)/shard_map/ppermute | solution.py:428
  178.1 6.0 %collective-permute-start.34 = (bf16[128,256]{1,0:T(8,128)(2,1)}, bf16[128,256]{1,0:T(8,128)(2,1)S(1)}, u32[]{:S(2)}, u32[]{:S(2)}) collective-permute-start(bf16[128,256]{1,0:T(8,128)(2,1)} %get-tuple-element.44.refs_0_), channel_id=1, source_target_pairs={{0,4},{1,5},{2,6},{3,7},{4,0},{5,1},{6,2},{7,3},{8,12},{9,13},{10,... | collective-permute-start | bytes 196616 | tf_op jit(solution)/shard_map/ppermute | solution.py:428
  180.5 5.7 %collective-permute-start.35 = (bf16[128,256]{1,0:T(8,128)(2,1)}, bf16[128,256]{1,0:T(8,128)(2,1)S(1)}, u32[]{:S(2)}, u32[]{:S(2)}) collective-permute-start(bf16[128,256]{1,0:T(8,128)(2,1)} %get-tuple-element.44.refs_0_), channel_id=1, source_target_pairs={{0,6},{1,7},{2,4},{3,5},{4,2},{5,3},{6,0},{7,1},{8,14},{9,15},{10,... | collective-permute-start | bytes 196616 | tf_op jit(solution)/shard_map/ppermute | solution.py:428
  182.3 3.9 %collective-permute-start.36 = (bf16[128,256]{1,0:T(8,128)(2,1)}, bf16[128,256]{1,0:T(8,128)(2,1)S(1)}, u32[]{:S(2)}, u32[]{:S(2)}) collective-permute-start(bf16[128,256]{1,0:T(8,128)(2,1)} %get-tuple-element.44.refs_0_), channel_id=1, source_target_pairs={{0,1},{1,0},{2,3},{3,2},{4,5},{5,4},{6,7},{7,6},{8,9},{9,8},{10,11... | collective-permute-start | bytes 196616 | tf_op jit(solution)/shard_map/ppermute | solution.py:433
  182.3 3.9 %collective-permute-start.37 = (bf16[128,256]{1,0:T(8,128)(2,1)S(1)}, bf16[128,256]{1,0:T(8,128)(2,1)S(1)}, u32[]{:S(2)}, u32[]{:S(2)}) collective-permute-start(bf16[128,256]{1,0:T(8,128)(2,1)S(1)} %collective-permute-done.33.refs_1_), channel_id=1, source_target_pairs={{0,1},{1,0},{2,3},{3,2},{4,5},{5,4},{6,7},{7,6},{8,9},{9,8},{10,11... | collective-permute-start | bytes 196616 | tf_op jit(solution)/shard_map/ppermute | solution.py:433
  184.0 2.2 collective-permute-start.38
  186.2 1.3 collective-permute-start.39
  191.8 10.8 %collective-permute-start.40 = (bf16[128,512]{1,0:T(8,128)(2,1)}, bf16[128,512]{1,0:T(8,128)(2,1)S(1)}, u32[]{:S(2)}, u32[]{:S(2)}) collective-permute-start(bf16[128,512]{1,0:T(8,128)(2,1)} %get-tuple-element.46), channel_id=1, source_target_pairs={{0,8},{8,16},{16,24},{24,32},{32,40},{40,48},{48,56},{56,64},{64,7... | collective-permute-start | bytes 393224 | tf_op jit(solution)/shard_map/ppermute | solution.py:438
  193.6 9.0 %collective-permute-start.41 = (bf16[128,512]{1,0:T(8,128)(2,1)}, bf16[128,512]{1,0:T(8,128)(2,1)S(1)}, u32[]{:S(2)}, u32[]{:S(2)}) collective-permute-start(bf16[128,512]{1,0:T(8,128)(2,1)} %get-tuple-element.47), channel_id=1, source_target_pairs={{0,120},{8,0},{16,8},{24,16},{32,24},{40,32},{48,40},{56,48},{64,5... | collective-permute-start | bytes 393224 | tf_op jit(solution)/shard_map/ppermute | solution.py:438
  195.1 7.0 %collective-permute-start.42 = (bf16[128,256]{1,0:T(8,128)(2,1)}, bf16[128,256]{1,0:T(8,128)(2,1)S(1)}, u32[]{:S(2)}, u32[]{:S(2)}) collective-permute-start(bf16[128,256]{1,0:T(8,128)(2,1)} %get-tuple-element.48), channel_id=1, source_target_pairs={{0,16},{8,24},{16,32},{24,40},{32,48},{40,56},{48,64},{56,72},{64,... | collective-permute-start | bytes 196616 | tf_op jit(solution)/shard_map/ppermute | solution.py:438
  195.2 7.4 %collective-permute-start.43 = (bf16[128,256]{1,0:T(8,128)(2,1)}, bf16[128,256]{1,0:T(8,128)(2,1)S(1)}, u32[]{:S(2)}, u32[]{:S(2)}) collective-permute-start(bf16[128,256]{1,0:T(8,128)(2,1)} %get-tuple-element.49), channel_id=1, source_target_pairs={{0,112},{8,120},{16,0},{24,8},{32,16},{40,24},{48,32},{56,40},{64,... | collective-permute-start | bytes 196616 | tf_op jit(solution)/shard_map/ppermute | solution.py:438
  203.7 11.8 %collective-permute-start.44 = (bf16[32,512]{1,0:T(8,128)(2,1)S(1)}, bf16[32,512]{1,0:T(8,128)(2,1)S(1)}, u32[]{:S(2)}, u32[]{:S(2)}) collective-permute-start(bf16[32,512]{1,0:T(8,128)(2,1)S(1)} %get-tuple-element.66), channel_id=1, source_target_pairs={{0,32},{8,40},{16,48},{24,56},{32,64},{40,72},{48,80},{56,88},{64,... | collective-permute-start | bytes 98312 | tf_op jit(solution)/shard_map/ppermute | solution.py:438
  207.0 12.8 %collective-permute-start.45 = (bf16[32,512]{1,0:T(8,128)(2,1)S(1)}, bf16[32,512]{1,0:T(8,128)(2,1)S(1)}, u32[]{:S(2)}, u32[]{:S(2)}) collective-permute-start(bf16[32,512]{1,0:T(8,128)(2,1)S(1)} %get-tuple-element.68), channel_id=1, source_target_pairs={{0,64},{8,72},{16,80},{24,88},{32,96},{40,104},{48,112},{56,120},{... | collective-permute-start | bytes 98312 | tf_op jit(solution)/shard_map/ppermute | solution.py:438
  211.8 8.0 %collective-permute-start.46 = (bf16[32,512]{1,0:T(8,128)(2,1)S(1)}, bf16[32,512]{1,0:T(8,128)(2,1)S(1)}, u32[]{:S(2)}, u32[]{:S(2)}) collective-permute-start(bf16[32,512]{1,0:T(8,128)(2,1)S(1)} %get-tuple-element.67), channel_id=1, source_target_pairs={{0,96},{8,104},{16,112},{24,120},{32,0},{40,8},{48,16},{56,24},{64... | collective-permute-start | bytes 98312 | tf_op jit(solution)/shard_map/ppermute | solution.py:438
  219.8 13.3 %collective-permute-start.47 = (bf16[32,512]{1,0:T(8,128)(2,1)S(1)}, bf16[32,512]{1,0:T(8,128)(2,1)S(1)}, u32[]{:S(2)}, u32[]{:S(2)}) collective-permute-start(bf16[32,512]{1,0:T(8,128)(2,1)S(1)} %fusion.7), channel_id=1, source_target_pairs={{0,32},{8,40},{16,48},{24,56},{32,64},{40,72},{48,80},{56,88},{64,... | collective-permute-start | bytes 98312 | tf_op jit(solution)/shard_map/ppermute | solution.py:438
  224.0 12.8 %collective-permute-start.48 = (bf16[32,512]{1,0:T(8,128)(2,1)S(1)}, bf16[32,512]{1,0:T(8,128)(2,1)S(1)}, u32[]{:S(2)}, u32[]{:S(2)}) collective-permute-start(bf16[32,512]{1,0:T(8,128)(2,1)S(1)} %fusion.7), channel_id=1, source_target_pairs={{0,64},{8,72},{16,80},{24,88},{32,96},{40,104},{48,112},{56,120},{... | collective-permute-start | bytes 98312 | tf_op jit(solution)/shard_map/ppermute | solution.py:438
  229.9 8.5 %collective-permute-start.49 = (bf16[32,512]{1,0:T(8,128)(2,1)S(1)}, bf16[32,512]{1,0:T(8,128)(2,1)S(1)}, u32[]{:S(2)}, u32[]{:S(2)}) collective-permute-start(bf16[32,512]{1,0:T(8,128)(2,1)S(1)} %fusion.7), channel_id=1, source_target_pairs={{0,96},{8,104},{16,112},{24,120},{32,0},{40,8},{48,16},{56,24},{64... | collective-permute-start | bytes 98312 | tf_op jit(solution)/shard_map/ppermute | solution.py:438
  238.5 11.2 %copy-start.5 = (bf16[128,512]{1,0:T(8,128)(2,1)}, bf16[128,512]{1,0:T(8,128)(2,1)S(1)}, u32[]{:S(2)}) copy-start(bf16[128,512]{1,0:T(8,128)(2,1)S(1)} %pad_maximum_fusion.1.own) | copy-start | bytes 393220
  238.5 15.7 %collective-permute-start.50 = (bf16[128,512]{1,0:T(8,128)(2,1)S(1)}, bf16[128,512]{1,0:T(8,128)(2,1)S(1)}, u32[]{:S(2)}, u32[]{:S(2)}) collective-permute-start(bf16[128,512]{1,0:T(8,128)(2,1)S(1)} %pad_maximum_fusion.1.own), channel_id=1, source_target_pairs={{0,120},{8,0},{16,8},{24,16},{32,24},{40,32},{48,40},{56,48},{64,5... | collective-permute-start | bytes 393224 | tf_op jit(solution)/shard_map/ppermute | solution.py:438
  241.5 12.7 %collective-permute-start.51 = (bf16[128,512]{1,0:T(8,128)(2,1)S(1)}, bf16[128,512]{1,0:T(8,128)(2,1)S(1)}, u32[]{:S(2)}, u32[]{:S(2)}) collective-permute-start(bf16[128,512]{1,0:T(8,128)(2,1)S(1)} %pad_maximum_fusion.1.own), channel_id=1, source_target_pairs={{0,8},{8,16},{16,24},{24,32},{32,40},{40,48},{48,56},{56,64},{64,7... | collective-permute-start | bytes 393224 | tf_op jit(solution)/shard_map/ppermute | solution.py:438
  241.5 12.7 %collective-permute-start.52 = (bf16[128,256]{1,0:T(8,128)(2,1)S(1)}, bf16[128,256]{1,0:T(8,128)(2,1)S(1)}, u32[]{:S(2)}, u32[]{:S(2)}) collective-permute-start(bf16[128,256]{1,0:T(8,128)(2,1)S(1)} %get-tuple-element.65), channel_id=1, source_target_pairs={{0,112},{8,120},{16,0},{24,8},{32,16},{40,24},{48,32},{56,40},{64,... | collective-permute-start | bytes 196616 | tf_op jit(solution)/shard_map/ppermute | solution.py:438
  245.2 8.9 %collective-permute-start.53 = (bf16[128,256]{1,0:T(8,128)(2,1)S(1)}, bf16[128,256]{1,0:T(8,128)(2,1)S(1)}, u32[]{:S(2)}, u32[]{:S(2)}) collective-permute-start(bf16[128,256]{1,0:T(8,128)(2,1)S(1)} %get-tuple-element.64), channel_id=1, source_target_pairs={{0,16},{8,24},{16,32},{24,40},{32,48},{40,56},{48,64},{56,72},{64,... | collective-permute-start | bytes 196616 | tf_op jit(solution)/shard_map/ppermute | solution.py:438
  (29 other events, 69.2 us)
